TPU v7x, 32 devices: a whole 2x2x4 slice. The times are simulated.
32 devices in a mesh: fs: 4 (over z), tp: 8 (over y, x, core).
Axes of the slice: x: 2, y: 2, z: 4, core: 2. Of those that a mesh axis runs over, the one named last changes fastest.
Arguments:
- tokens: bfloat16 [1024, 1344], P('fs'), may hold values from -6 to 6
- cotangent: bfloat16 [1024, 1344], P('fs'), may hold values from -8 to 8
- gate_weight: bfloat16 [1344, 3072], P('fs', 'tp'), may hold values from -0.15625 to 0.15625
- up_weight: bfloat16 [1344, 3072], P('fs', 'tp'), may hold values from -0.15625 to 0.15625
- down_weight: bfloat16 [3072, 1344], P('tp', 'fs'), may hold values from -0.109375 to 0.109375
Outputs:
- input_grad: bfloat16 [1024, 1344], P('fs')
- down_grad: float32 [3072, 1344], P('tp', 'fs')
All inputs are finite; a program needn't handle non-finite values.
Results may differ from a plain program's by a relative error of at most 0.013.
Values may be sent and summed in bfloat16 or wider, within the bound.
A program may use at most 64 MiB of HBM per device.

v0:
```python
import functools

import jax
import jax.numpy as jnp
from jax import lax
from jax.experimental import pallas as pl
from jax.experimental.pallas import tpu as pltpu
from jax.sharding import PartitionSpec as P

LANES = 128
SUB = 16
BF16 = jnp.bfloat16
F32 = jnp.float32


def contract_rows(left, right):
    return lax.dot_general(
        left, right, (((0,), (0,)), ((), ())), preferred_element_type=jnp.float32
    )


def contract_cols(left, right):
    return lax.dot_general(
        left, right, (((1,), (1,)), ((), ())), preferred_element_type=jnp.float32
    )


def send_down(hidden, cotangent):
    return lax.psum_scatter(
        contract_rows(cotangent, hidden), "fs", scatter_dimension=0, tiled=True
    ).T


def per_device_plain(tokens, cotangent, gate_weight, up_weight, down_weight):
    whole_gate, whole_up, whole_down = (
        lax.all_gather(gate_weight, "fs", axis=0, tiled=True),
        lax.all_gather(up_weight, "fs", axis=0, tiled=True),
        lax.all_gather(down_weight, "fs", axis=1, tiled=True),
    )
    gate_pre = jnp.dot(tokens, whole_gate, preferred_element_type=jnp.float32)
    up_pre = jnp.dot(tokens, whole_up, preferred_element_type=jnp.float32)
    hidden_grad = contract_cols(cotangent, whole_down)
    sigmoid_gate = jax.nn.sigmoid(gate_pre)
    activated = gate_pre * sigmoid_gate
    hidden = (activated * up_pre).astype(jnp.bfloat16)
    gate_pre_grad = (
        hidden_grad * up_pre * sigmoid_gate * (1.0 + gate_pre * (1.0 - sigmoid_gate))
    ).astype(jnp.bfloat16)
    up_pre_grad = (hidden_grad * activated).astype(jnp.bfloat16)
    partial_value = contract_cols(gate_pre_grad, whole_gate) + contract_cols(up_pre_grad, whole_up)
    input_grad = lax.psum(partial_value.astype(jnp.bfloat16), "tp")
    down_grad = send_down(hidden, cotangent)
    return (input_grad, down_grad)


def kernel(n, tok_ref, cot_ref, gate_ref, up_ref, down_ref, dx_out, dg_out,
           weights, tok, cot, dxacc, part, rsr, rss, rx1, rx2, rx3, tx1, tx2, tx3, ybuf,
           ag_send, ag_recv, rs_send, rs_recv, ar_send, ar_recv, loc_sem):
    z = lax.axis_index("fs")
    b = lax.axis_index("tp")
    depth, rows = tok_ref.shape
    shard, ff = gate_ref.shape
    chunks = ff // LANES
    core = lax.rem(b, 2)
    m2 = 2 + 2 * core
    m3 = 6 - m2
    bit2 = lax.rem(b // m2, 2)
    bit3 = lax.rem(b // m3, 2)
    p1 = b + 1 - 2 * core
    p2 = b + m2 * (1 - 2 * bit2)
    p3 = b + m3 * (1 - 2 * bit3)
    has_left = z > 0
    has_right = z < n - 1

    def z_id(step):
        return {"fs": z + step}

    barrier = pltpu.get_barrier_semaphore()
    for partner in (p1, p2, p3):
        pl.semaphore_signal(barrier, inc=1, device_id={"tp": partner},
                            device_id_type=pl.DeviceIdType.MESH)
    for step, there in ((-1, has_left), (1, has_right)):
        @pl.when(there)
        def _():
            pl.semaphore_signal(barrier, inc=1, device_id=z_id(step),
                                device_id_type=pl.DeviceIdType.MESH)
    peers = 3 + lax.div(z + n - 1, n) + lax.div(2 * n - 2 - z, n)
    pl.semaphore_wait(barrier, peers)

    def slot(c, s, kind):
        r = pl.ds(pl.multiple_of(s * shard, SUB), shard)
        return weights.at[r, pl.ds((3 * c + kind) * LANES, LANES)]

    def own(c, kind):
        return (gate_ref, up_ref, down_ref)[kind].at[:, pl.ds(c * LANES, LANES)]

    def ag_copy(src, c, s, kind, side):
        step = 1 if side else -1
        return pltpu.make_async_remote_copy(
            src_ref=src, dst_ref=slot(c, s, kind),
            send_sem=ag_send.at[side, c, s, kind], recv_sem=ag_recv.at[c, s, kind],
            device_id=z_id(step), device_id_type=pl.DeviceIdType.MESH)

    def send_own(c):
        for side, there in ((0, has_left), (1, has_right)):
            @pl.when(there)
            def _():
                for kind in range(3):
                    ag_copy(own(c, kind), c, z, kind, side).start()

    def gather(c):
        for d in range(1, n):
            for side in (0, 1):
                s = z - d if side == 0 else z + d
                here = (z >= d) if side == 0 else (z + d <= n - 1)
                onward = has_right if side == 0 else has_left
                @pl.when(here)
                def _():
                    for kind in range(3):
                        src = slot(c, s, kind)
                        ag_copy(src, c, s, kind, 1 - side).wait_recv()
                        @pl.when(onward)
                        def _():
                            ag_copy(src, c, s, kind, 1 - side).start()

    def local_copy(c, kind):
        return pltpu.make_async_copy(own(c, kind), slot(c, z, kind), loc_sem.at[c, kind])

    for c in range(min(2, chunks)):
        send_own(c)
    for c in range(chunks):
        for kind in range(3):
            local_copy(c, kind).start()
    tok[...] = tok_ref[...].T
    cot[...] = cot_ref[...].T

    def rs_copy(c, k, side):
        return pltpu.make_async_remote_copy(
            src_ref=rss.at[side, c, k], dst_ref=rsr.at[side, c, k],
            send_sem=rs_send.at[side, c, k], recv_sem=rs_recv.at[side, c, k],
            device_id=z_id(1 if side else -1), device_id_type=pl.DeviceIdType.MESH)

    def rs_targets(side):
        return range(n - 1, 0, -1) if side else range(n - 1)

    def rs_start(c):
        for side, end in ((1, z == 0), (0, z == n - 1)):
            @pl.when(end)
            def _():
                for k in rs_targets(side):
                    rss[side, c, k] = part[c, k].astype(BF16)
                    rs_copy(c, k, side).start()

    def rs_mid(c):
        for side, middle in ((1, has_left), (0, has_right)):
            for k in rs_targets(side):
                ahead = (k > z) if side else (k < z)
                @pl.when(jnp.logical_and(middle, ahead))
                def _():
                    rs_copy(c, k, side).wait_recv()
                    rss[side, c, k] = (part[c, k] + rsr[side, c, k].astype(F32)).astype(BF16)
                    rs_copy(c, k, side).start()

    def rs_final(c):
        r = pl.ds(c * LANES, LANES)
        dg_out[:, r] = part[c, z]
        for side, there in ((1, has_left), (0, has_right)):
            @pl.when(there)
            def _():
                rs_copy(c, z, side).wait_recv()
                dg_out[:, r] += rsr[side, c, z].astype(F32)

    def ar_copy(i, src, dst, partner):
        return pltpu.make_async_remote_copy(
            src_ref=src, dst_ref=dst, send_sem=ar_send.at[i], recv_sem=ar_recv.at[i],
            device_id={"tp": partner}, device_id_type=pl.DeviceIdType.MESH)

    half, quarter, lanes = depth // 2, depth // 4, rows // 2
    lo1 = core * half
    other1 = (1 - core) * half
    lo2 = lo1 + bit2 * quarter
    other2 = lo1 + (1 - bit2) * quarter
    mine3 = pl.ds(pl.multiple_of(bit3 * lanes, LANES), lanes)
    other3 = pl.ds(pl.multiple_of((1 - bit3) * lanes, LANES), lanes)

    def at(lo, size):
        return pl.ds(pl.multiple_of(lo, SUB), size)

    ar1 = ar_copy(0, tx1, rx1, p1)
    ar2 = ar_copy(1, tx2, rx2, p2)
    ar3 = ar_copy(2, tx3, rx3, p3)

    for c in range(chunks):
        gather(c)
        if c + 2 < chunks:
            send_own(c + 2)
        if c >= 2:
            rs_mid(c - 2)
        for kind in range(3):
            local_copy(c, kind).wait()
        w = weights[:, 3 * c * LANES:(3 * c + 2) * LANES]
        pre = jnp.dot(tok[...], w, preferred_element_type=F32)
        hg = jnp.dot(cot[...], weights[:, (3 * c + 2) * LANES:(3 * c + 3) * LANES],
                     preferred_element_type=F32)
        gate_pre, up_pre = pre[:, :LANES], pre[:, LANES:]
        sig = jax.nn.sigmoid(gate_pre)
        act = gate_pre * sig
        hidden = (act * up_pre).astype(BF16)
        dgu = jnp.concatenate(
            [(hg * up_pre * sig * (1.0 + gate_pre * (1.0 - sig))).astype(BF16),
             (hg * act).astype(BF16)], axis=1)
        if c == 0:
            dxacc[...] = contract_cols(w, dgu)
        else:
            dxacc[...] += contract_cols(w, dgu)
        if c == chunks - 1:
            tx1[...] = dxacc[at(other1, half), :].astype(BF16)
            ar1.start()
        for k in range(n):
            part[c, k] = jnp.dot(cot_ref[k * shard:(k + 1) * shard, :], hidden,
                                 preferred_element_type=F32)
        rs_start(c)

    ar1.wait_recv()
    tx2[...] = (dxacc[at(other2, quarter), :]
                + rx1[at(other2 - lo1, quarter), :].astype(F32)).astype(BF16)
    ar2.start()
    dxacc[at(lo2, quarter), :] += rx1[at(lo2 - lo1, quarter), :].astype(F32)
    ar2.wait_recv()
    q = at(lo2, quarter)
    tx3[...] = (dxacc[q, other3] + rx2[:, other3].astype(F32)).astype(BF16)
    ar3.start()
    kept = dxacc[q, mine3] + rx2[:, mine3].astype(F32)
    ar3.wait_recv()
    ybuf[q, mine3] = (kept + rx3[...].astype(F32)).astype(BF16)
    backs = []
    whole = pl.ds(0, rows)
    for i, r, l, partner in ((3, q, mine3, p3), (4, q, whole, p2), (5, at(lo1, half), whole, p1)):
        own_rows = ybuf.at[r, l]
        back = ar_copy(i, own_rows, own_rows, partner)
        back.start()
        back.wait_recv()
        backs.append(back)
    dx_out[...] = ybuf[...]

    for c in range(max(0, chunks - 2), chunks):
        rs_mid(c)
    for c in range(chunks):
        rs_final(c)

    for copy in [ar1, ar2, ar3] + backs:
        copy.wait_send()
    for side, there in ((0, has_left), (1, has_right)):
        @pl.when(there)
        def _():
            for c in range(chunks):
                for kind in range(3):
                    ag_copy(own(c, kind), c, z, kind, side).wait_send()
    for d in range(1, n):
        for side in (0, 1):
            s = z - d if side == 0 else z + d
            here = (z >= d) if side == 0 else (z + d <= n - 1)
            onward = has_right if side == 0 else has_left
            @pl.when(jnp.logical_and(here, onward))
            def _():
                for c in range(chunks):
                    for kind in range(3):
                        ag_copy(slot(c, s, kind), c, s, kind, 1 - side).wait_send()
    for side in (0, 1):
        for k in rs_targets(side):
            sent = (k > z) if side else (k < z)
            @pl.when(sent)
            def _():
                for c in range(chunks):
                    rs_copy(c, k, side).wait_send()


def per_device_kernel(n, tokens, cotangent, gate_weight, up_weight, down_weight):
    rows, depth = tokens.shape
    shard, ff = gate_weight.shape
    chunks = ff // LANES
    vmem = pl.BlockSpec(memory_space=pltpu.VMEM)
    dma = pltpu.SemaphoreType.DMA
    dx, dg = pl.pallas_call(
        functools.partial(kernel, n),
        out_shape=(jax.ShapeDtypeStruct((depth, rows), BF16),
                   jax.ShapeDtypeStruct((shard, ff), F32)),
        in_specs=[vmem] * 5,
        out_specs=(vmem, vmem),
        scratch_shapes=[
            pltpu.VMEM((depth, 3 * ff), BF16),
            pltpu.VMEM((rows, depth), BF16),
            pltpu.VMEM((rows, depth), BF16),
            pltpu.VMEM((depth, rows), F32),
            pltpu.VMEM((chunks, n, shard, LANES), F32),
            pltpu.VMEM((2, chunks, n, shard, LANES), BF16),
            pltpu.VMEM((2, chunks, n, shard, LANES), BF16),
            pltpu.VMEM((depth // 2, rows), BF16),
            pltpu.VMEM((depth // 4, rows), BF16),
            pltpu.VMEM((depth // 4, rows // 2), BF16),
            pltpu.VMEM((depth // 2, rows), BF16),
            pltpu.VMEM((depth // 4, rows), BF16),
            pltpu.VMEM((depth // 4, rows // 2), BF16),
            pltpu.VMEM((depth, rows), BF16),
            dma((2, chunks, n, 3)), dma((chunks, n, 3)),
            dma((2, chunks, n)), dma((2, chunks, n)),
            dma((6,)), dma((6,)), dma((chunks, 3)),
        ],
        compiler_params=pltpu.CompilerParams(
            collective_id=0, has_side_effects=True, vmem_limit_bytes=56 * 2**20),
    )(tokens.T, cotangent.T, gate_weight, up_weight, down_weight.T)
    return dx.T, dg.T


def solution(mesh):
    n, tp = mesh.shape["fs"], mesh.shape["tp"]

    def per_device(tokens, cotangent, gate_weight, up_weight, down_weight):
        rows = tokens.shape[0]
        shard, ff = gate_weight.shape
        args = (tokens, cotangent, gate_weight, up_weight, down_weight)
        fits = (tp == 8 and 2 <= n <= 8 and rows % (2 * LANES) == 0 and tokens.shape[1] % (4 * SUB) == 0 and rows <= 512
                and shard % SUB == 0 and ff % LANES == 0)
        return per_device_kernel(n, *args) if fits else per_device_plain(*args)

    placed = (P("fs", None), P("fs", None), P("fs", "tp"), P("fs", "tp"), P("tp", "fs"))
    return jax.shard_map(
        per_device,
        mesh=mesh,
        in_specs=placed,
        out_specs=(P("fs", None), P("tp", "fs")),
        check_vma=False,
    )
```

profile of v0, /device:TPU:0, one launch (start us, length us, event | category | flops | bytes accessed | tf_op | source)
XLA Modules:
  0.0 90.8 jit_solution(9015037794264019529)
XLA Ops:
  0.6 87.4 %shard_map.68 = (bf16[1344,256]{1,0:T(8,128)(2,1)}, f32[336,384]{1,0:T(8,128)}) custom-call(bf16[1344,256]{1,0:T(8,128)(2,1)} %bitcast.5, bf16[1344,256]{1,0:T(8,128)(2,1)} %bitcast.6, bf16[336,384]{1,0:T(8,128)(2,1)} %gate_ref.1, bf16[336,384]{1,0:T(8,128)(2,1)} %up_ref.1, bf16[336,384]{1,0:T(8,128)(2,1)} %bitcast.9), custom_call_target="tpu_custom_call" | custom-call | tf_op jit(solution)/shard_map/pallas_call | solution.py:284
  88.0 0.0 copy-start
  88.0 2.0 %copy.9 = bf16[256,1344]{0,1:T(8,128)(2,1)} copy(bf16[256,1344]{0,1:T(8,128)(2,1)} %bitcast.7) | data formatting | bytes 1376256
  90.0 0.0 copy-done
  90.1 0.8 copy.10
Async XLA Ops:
  88.0 2.1 %copy-start = (f32[336,384]{1,0:T(8,128)S(1)}, f32[336,384]{1,0:T(8,128)}, u32[]{:S(2)}) copy-start(f32[336,384]{1,0:T(8,128)} %get-tuple-element.5) | copy-start | bytes 1548292
where the time goes:
time: 91.3 us; the launch traced here: 90.8 us
  Pallas kernels  87.4 us (96%)
  local copies, waits for them, and re-layouts  2.84 us (3%)
    pallas_call x1, Pallas kernels, per_device_kernel(): pl.pallas_call(functools.partial(kernel, n), out_shape=(jax.ShapeDtypeStr...  87.4 us
    unnamed x4, local copies, waits for them, and re-layouts  2.84 us

commit v1 on v0

v1 whole, which is shorter than its diff:
```python
import functools

import jax
import jax.numpy as jnp
from jax import lax
from jax.experimental import pallas as pl
from jax.experimental.pallas import tpu as pltpu
from jax.sharding import PartitionSpec as P

LANES = 128
SUB = 16
BF16 = jnp.bfloat16
F32 = jnp.float32


def contract_rows(left, right):
    return lax.dot_general(
        left, right, (((0,), (0,)), ((), ())), preferred_element_type=jnp.float32
    )


def contract_cols(left, right):
    return lax.dot_general(
        left, right, (((1,), (1,)), ((), ())), preferred_element_type=jnp.float32
    )


def send_down(hidden, cotangent):
    return lax.psum_scatter(
        contract_rows(cotangent, hidden), "fs", scatter_dimension=0, tiled=True
    ).T


def per_device_plain(tokens, cotangent, gate_weight, up_weight, down_weight):
    whole_gate, whole_up, whole_down = (
        lax.all_gather(gate_weight, "fs", axis=0, tiled=True),
        lax.all_gather(up_weight, "fs", axis=0, tiled=True),
        lax.all_gather(down_weight, "fs", axis=1, tiled=True),
    )
    gate_pre = jnp.dot(tokens, whole_gate, preferred_element_type=jnp.float32)
    up_pre = jnp.dot(tokens, whole_up, preferred_element_type=jnp.float32)
    hidden_grad = contract_cols(cotangent, whole_down)
    sigmoid_gate = jax.nn.sigmoid(gate_pre)
    activated = gate_pre * sigmoid_gate
    hidden = (activated * up_pre).astype(jnp.bfloat16)
    gate_pre_grad = (
        hidden_grad * up_pre * sigmoid_gate * (1.0 + gate_pre * (1.0 - sigmoid_gate))
    ).astype(jnp.bfloat16)
    up_pre_grad = (hidden_grad * activated).astype(jnp.bfloat16)
    partial_value = contract_cols(gate_pre_grad, whole_gate) + contract_cols(up_pre_grad, whole_up)
    input_grad = lax.psum(partial_value.astype(jnp.bfloat16), "tp")
    down_grad = send_down(hidden, cotangent)
    return (input_grad, down_grad)


def kernel(n, tok_ref, cot_ref, gate_ref, up_ref, down_ref, dx_out, dg_out,
           weights, tok, cot, ptok, pcot, dxacc, hid, dgp, dgs, dgr, dgf,
           t1s, t1r, t2s, t2r, t3s, t3r, ybuf,
           z_send, s_send, w_recv, loc_sem, tk_send, tk_recv, hid_send, hid_recv,
           dg_send, dg_recv, dgf_send, dgf_recv, t1_send, t1_recv, t2_send, t2_recv,
           t3_send, t3_recv, y_send, y_recv, yd_send, yd_recv):
    z = lax.axis_index("fs")
    b = lax.axis_index("tp")
    depth, rows = tok_ref.shape
    shard, ff = gate_ref.shape
    chunks = ff // LANES
    parts = t2s.shape[1]
    piece = shard // parts
    half_rows = rows // 2
    core = lax.rem(b, 2)
    col = lax.div(b, 2)
    cx = lax.rem(col, 2)
    cy = lax.div(col, 2)
    side = lax.div(z, 2)
    home = core == side
    away = core != side
    near = jnp.logical_or(z == 1, z == 2)
    end = jnp.logical_not(near)
    zodd = lax.rem(z, 2)
    sib = b + 1 - 2 * core
    bx = b + 2 * (1 - 2 * cx)
    by = b + 4 * (1 - 2 * cy)
    zs = z + 1 - 2 * zodd
    zp = lax.rem(z + 2, 4)
    zn = 2 - side
    zf = 3 - 3 * side
    me = jnp.where(home, 0, 1)
    col_x = 2 * cy + 1 - cx
    col_y = 2 * (1 - cy) + cx
    col_d = 2 * (1 - cy) + 1 - cx

    barrier = pltpu.get_barrier_semaphore()

    def greet(fs, tp):
        pl.semaphore_signal(barrier, inc=1, device_id={"fs": fs, "tp": tp},
                            device_id_type=pl.DeviceIdType.MESH)

    greet(z, sib)
    greet(z, bx)
    greet(z, by)
    for step in range(1, n):
        greet(lax.rem(z + step, n), b)
        greet(lax.rem(z + step, n), sib)
    pl.semaphore_wait(barrier, 3 + 2 * (n - 1))

    def remote(src, dst, send, recv, fs, tp):
        return pltpu.make_async_remote_copy(
            src_ref=src, dst_ref=dst, send_sem=send, recv_sem=recv,
            device_id={"fs": fs, "tp": tp}, device_id_type=pl.DeviceIdType.MESH)

    def rows_of(k, count=1):
        return pl.ds(pl.multiple_of(k * shard, SUB), count * shard)

    def slot(c, k, kind):
        return weights.at[rows_of(k), pl.ds((3 * c + kind) * LANES, LANES)]

    def own(c, kind):
        return (gate_ref, up_ref, down_ref)[kind].at[:, pl.ds(c * LANES, LANES)]

    def w_copy(src, c, k, kind, fs):
        return remote(src, slot(c, k, kind), z_send.at[c, k, kind], w_recv.at[c, k, kind], fs, b)

    def sib_copy(src, c, k, kind):
        return remote(src, slot(c, k, kind), s_send.at[c, k, kind], w_recv.at[c, k, kind], z, sib)

    def local_copy(c, kind):
        return pltpu.make_async_copy(own(c, kind), slot(c, z, kind), loc_sem.at[c, kind])

    every = [(c, kind) for c in range(chunks) for kind in range(3)]
    mine_q = rows_of(col)
    far_rows = rows_of(2 * side, 2)

    def tk_copy(i, src, dst, fs, tp):
        return remote(src, dst, tk_send.at[i], tk_recv.at[i], fs, tp)

    tok_hop = tk_copy(0, tok_ref.at[mine_q], ptok.at[mine_q], zp, b)
    cot_hop = tk_copy(1, cot_ref.at[mine_q], pcot.at[mine_q], zp, sib)

    def spread(i, buf, q, tp):
        return tk_copy(i, buf.at[rows_of(q)], buf.at[rows_of(q)], z, tp)

    give = tk_copy(8, pcot.at[far_rows], pcot.at[far_rows], z, sib)

    @pl.when(home)
    def _():
        remote(tok_ref.at[mine_q], ptok.at[mine_q], tk_send.at[0], tk_recv.at[0], zp, b).start()
        for c, kind in every:
            w_copy(own(c, kind), c, z, kind, zs).start()
            sib_copy(own(c, kind), c, z, kind).start()
            local_copy(c, kind).start()
        tok[...] = tok_ref[...].T
        cot[...] = cot_ref[...].T

    @pl.when(away)
    def _():
        remote(cot_ref.at[mine_q], pcot.at[mine_q], tk_send.at[1], tk_recv.at[1], zp, sib).start()
        for c, kind in every:
            w_copy(own(c, kind), c, z, kind, zn).start()
        tok_hop.wait_recv()
        spread(2, ptok, col, bx).start()
        spread(3, ptok, col, by).start()
        cot_hop.wait_recv()
        spread(4, pcot, col, bx).start()
        spread(5, pcot, col, by).start()
        spread(2, ptok, col_x, bx).wait_recv()
        spread(6, ptok, col_x, by).start()
        spread(5, pcot, col_y, by).wait_recv()
        spread(7, pcot, col_y, bx).start()
        spread(3, ptok, col_y, by).wait_recv()
        spread(6, ptok, col_d, by).wait_recv()
        tok[...] = ptok[...].T
        spread(4, pcot, col_x, bx).wait_recv()
        spread(7, pcot, col_d, bx).wait_recv()
        give.start()
        cot[...] = pcot[...].T

    others = (zs, zn, zf)

    def gather(c):
        @pl.when(home)
        def _():
            for kind in range(3):
                for i, k in enumerate(others):
                    w_copy(slot(c, k, kind), c, k, kind, zs).wait_recv()
                    if i:
                        @pl.when(near)
                        def _():
                            w_copy(slot(c, k, kind), c, k, kind, zs).start()
                    sib_copy(slot(c, k, kind), c, k, kind).start()
            for kind in range(3):
                local_copy(c, kind).wait()

        @pl.when(away)
        def _():
            for kind in range(3):
                for k in range(n):
                    sib_copy(slot(c, k, kind), c, k, kind).wait_recv()

    def hid_copy(c):
        return remote(hid.at[me, c], hid.at[me, c], hid_send.at[c], hid_recv.at[c], z, sib)

    def dg_home(c):
        return remote(dgs.at[c, 0], dgr.at[c, 0], dg_send.at[c], dg_recv.at[c], zs, b)

    def dg_away(c):
        return remote(dgs.at[c], dgr.at[c], dg_send.at[c], dg_recv.at[c], zs, b)

    def dg_far(c, i):
        return remote(dgs.at[c, i], dgf.at[c], dgf_send.at[c, i], dgf_recv.at[c],
                      2 * (1 - side) + i, sib)

    def lanes_of(c):
        return pl.ds(c * LANES, LANES)

    def down_part(c):
        hid_copy(c).wait_recv()
        for i in range(2):
            k = rows_of(2 * core + i)
            value = (jnp.dot(cot_ref[k, :], hid[0, c], preferred_element_type=F32)
                     + jnp.dot(pcot[k, :], hid[1, c], preferred_element_type=F32))

            @pl.when(jnp.logical_and(home, zodd == i))
            def _():
                dg_out[:, lanes_of(c)] = value

            @pl.when(jnp.logical_and(home, zodd != i))
            def _():
                dgs[c, 0] = value.astype(BF16)

            @pl.when(jnp.logical_and(away, near))
            def _():
                dgp[c, i] = value

            @pl.when(jnp.logical_and(away, end))
            def _():
                dgs[c, i] = value.astype(BF16)

        @pl.when(home)
        def _():
            dg_home(c).start()

        @pl.when(jnp.logical_and(away, end))
        def _():
            dg_away(c).start()

    def down_mid(c):
        @pl.when(jnp.logical_and(away, near))
        def _():
            dg_away(c).wait_recv()
            for i in range(2):
                dgs[c, i] = (dgp[c, i] + dgr[c, i].astype(F32)).astype(BF16)
                dg_far(c, i).start()

    def down_final(c):
        @pl.when(home)
        def _():
            dg_home(c).wait_recv()
            dg_out[:, lanes_of(c)] += dgr[c, 0].astype(F32)

        @pl.when(away)
        def _():
            dg_far(c, 0).wait_recv()
            dg_out[:, lanes_of(c)] = dgf[c].astype(F32)

    low, high = slice(0, half_rows), slice(half_rows, rows)
    halves = (low, high)

    def t1_copy(i, step):
        return remote(t1s.at[i, step], t1r.at[i, step], t1_send.at[i, step], t1_recv.at[i, step],
                      z, bx if i == 0 else by)

    def t2_copy(i, q):
        return remote(t2s.at[i, q], t2r.at[i, q], t2_send.at[i, q], t2_recv.at[i, q],
                      z, by if i == 0 else bx)

    def t3_copy(q):
        return remote(t3s.at[q], t3r.at[q], t3_send.at[q], t3_recv.at[q], zp, b)

    def strip(k, q):
        return pl.ds(pl.multiple_of(k * shard + q * piece, SUB), piece)

    def y_copy(i, k, q, tp):
        ref = ybuf.at[strip(k, q)]
        return remote(ref, ref, y_send.at[i, q], y_recv.at[i, q], z, tp)

    def y_half(i, k, q, tp):
        ref = ybuf.at[strip(k, q), pl.ds(i * half_rows, half_rows)]
        return remote(ref, ref, yd_send.at[i, q], yd_recv.at[i, q], z, tp)

    def y_sib(i, k, q):
        ref = ybuf.at[strip(k, q)]
        return remote(ref, ref, y_send.at[2 + i, q], y_recv.at[2 + i, q], z, sib)

    for c in range(chunks):
        gather(c)
        w = weights[:, 3 * c * LANES:(3 * c + 2) * LANES]
        pre = jnp.dot(tok[...], w, preferred_element_type=F32)
        hg = jnp.dot(cot[...], weights[:, (3 * c + 2) * LANES:(3 * c + 3) * LANES],
                     preferred_element_type=F32)
        gate_pre, up_pre = pre[:, :LANES], pre[:, LANES:]
        sig = jax.nn.sigmoid(gate_pre)
        act = gate_pre * sig
        hid[me, c] = (act * up_pre).astype(BF16)
        hid_copy(c).start()
        dgu = jnp.concatenate(
            [(hg * up_pre * sig * (1.0 + gate_pre * (1.0 - sig))).astype(BF16),
             (hg * act).astype(BF16)], axis=1)
        if c == 0:
            dxacc[...] = contract_cols(w, dgu)
        elif c < chunks - 1:
            dxacc[...] += contract_cols(w, dgu)
        if c == 0:
            @pl.when(home)
            def _():
                give.wait_recv()
        if c < chunks - 1:
            down_part(c)
        if 0 < c < chunks - 1:
            down_mid(c - 1)
        if c == chunks - 1:
            for k, sends in ((col_d, ((0, 0), (1, 0))), (col_x, ((0, 1),)), (col_y, ((1, 1),)), (col, ())):
                r = rows_of(k)
                value = contract_cols(weights[r, 3 * c * LANES:(3 * c + 2) * LANES], dgu)
                if c:
                    value = value + dxacc[r, :]
                if k is not col_d:
                    dxacc[r, :] = value
                for i, step in sends:
                    t1s[i, step] = value[:, halves[i]].astype(BF16)
                    t1_copy(i, step).start()

    down_part(chunks - 1)
    t1_copy(0, 0).wait_recv()
    t1_copy(1, 0).wait_recv()
    for q in range(parts):
        inner = slice(q * piece, (q + 1) * piece)
        for i, k in ((0, col_y), (1, col_x)):
            t2s[i, q] = (dxacc[strip(k, q), halves[i]] + t1r[i, 0, inner].astype(F32)).astype(BF16)
            t2_copy(i, q).start()
    t1_copy(0, 1).wait_recv()
    t1_copy(1, 1).wait_recv()
    for q in range(parts):
        inner = slice(q * piece, (q + 1) * piece)
        for i in range(2):
            dxacc[strip(col, q), halves[i]] += t1r[i, 1, inner].astype(F32)
    for q in range(parts):
        for i in range(2):
            t2_copy(i, q).wait_recv()
            dxacc[strip(col, q), halves[i]] += t2r[i, q].astype(F32)

        @pl.when(away)
        def _():
            t3s[q] = dxacc[strip(col, q), :].astype(BF16)
            t3_copy(q).start()
    for c in range(max(0, chunks - 2), chunks):
        down_mid(c)

    @pl.when(home)
    def _():
        for q in range(parts):
            t3_copy(q).wait_recv()
            ybuf[strip(col, q), :] = (dxacc[strip(col, q), :] + t3r[q].astype(F32)).astype(BF16)
            y_copy(0, col, q, bx).start()
            y_copy(1, col, q, by).start()
            y_sib(0, col, q).start()
        for q in range(parts):
            y_copy(0, col_x, q, bx).wait_recv()
            y_half(0, col_x, q, by).start()
            y_sib(1, col_x, q).start()
            y_copy(1, col_y, q, by).wait_recv()
            y_half(1, col_y, q, bx).start()
            y_sib(2, col_y, q).start()
        for q in range(parts):
            y_half(0, col_d, q, by).wait_recv()
            y_half(1, col_d, q, bx).wait_recv()
            y_sib(3, col_d, q).start()

    for c in range(chunks):
        down_final(c)

    @pl.when(away)
    def _():
        for q in range(parts):
            for i, k in enumerate((col, col_x, col_y, col_d)):
                y_sib(i, k, q).wait_recv()
    dx_out[...] = ybuf[...]

    @pl.when(home)
    def _():
        tok_hop.wait_send()
        for c, kind in every:
            w_copy(own(c, kind), c, z, kind, zs).wait_send()
            sib_copy(own(c, kind), c, z, kind).wait_send()
            for i, k in enumerate(others):
                sib_copy(slot(c, k, kind), c, k, kind).wait_send()
                if i:
                    @pl.when(near)
                    def _():
                        w_copy(slot(c, k, kind), c, k, kind, zs).wait_send()
        for c in range(chunks):
            dg_home(c).wait_send()
        for q in range(parts):
            y_copy(0, col, q, bx).wait_send()
            y_copy(1, col, q, by).wait_send()
            y_half(0, col_x, q, by).wait_send()
            y_half(1, col_y, q, bx).wait_send()
            for i, k in enumerate((col, col_x, col_y, col_d)):
                y_sib(i, k, q).wait_send()

    @pl.when(away)
    def _():
        cot_hop.wait_send()
        for c, kind in every:
            w_copy(own(c, kind), c, z, kind, zn).wait_send()
        spread(2, ptok, col, bx).wait_send()
        spread(3, ptok, col, by).wait_send()
        spread(4, pcot, col, bx).wait_send()
        spread(5, pcot, col, by).wait_send()
        spread(6, ptok, col_x, by).wait_send()
        spread(7, pcot, col_y, bx).wait_send()
        give.wait_send()
        for q in range(parts):
            t3_copy(q).wait_send()
        for c in range(chunks):
            @pl.when(end)
            def _():
                dg_away(c).wait_send()

            @pl.when(near)
            def _():
                for i in range(2):
                    dg_far(c, i).wait_send()

    for c in range(chunks):
        hid_copy(c).wait_send()
    for i in range(2):
        for step in range(2):
            t1_copy(i, step).wait_send()
        for q in range(parts):
            t2_copy(i, q).wait_send()


def per_device_kernel(n, tokens, cotangent, gate_weight, up_weight, down_weight):
    rows, depth = tokens.shape
    shard, ff = gate_weight.shape
    chunks = ff // LANES
    parts = next(p for p in (3, 2, 1) if shard % (p * SUB) == 0)
    piece = shard // parts
    vmem = pl.BlockSpec(memory_space=pltpu.VMEM)
    dma = pltpu.SemaphoreType.DMA
    dx, dg = pl.pallas_call(
        functools.partial(kernel, n),
        out_shape=(jax.ShapeDtypeStruct((depth, rows), BF16),
                   jax.ShapeDtypeStruct((shard, ff), F32)),
        in_specs=[vmem] * 5,
        out_specs=(vmem, vmem),
        scratch_shapes=[
            pltpu.VMEM((depth, 3 * ff), BF16),
            pltpu.VMEM((rows, depth), BF16),
            pltpu.VMEM((rows, depth), BF16),
            pltpu.VMEM((depth, rows), BF16),
            pltpu.VMEM((depth, rows), BF16),
            pltpu.VMEM((depth, rows), F32),
            pltpu.VMEM((2, chunks, rows, LANES), BF16),
            pltpu.VMEM((chunks, 2, shard, LANES), F32),
            pltpu.VMEM((chunks, 2, shard, LANES), BF16),
            pltpu.VMEM((chunks, 2, shard, LANES), BF16),
            pltpu.VMEM((chunks, shard, LANES), BF16),
            pltpu.VMEM((2, 2, shard, rows // 2), BF16),
            pltpu.VMEM((2, 2, shard, rows // 2), BF16),
            pltpu.VMEM((2, parts, piece, rows // 2), BF16),
            pltpu.VMEM((2, parts, piece, rows // 2), BF16),
            pltpu.VMEM((parts, piece, rows), BF16),
            pltpu.VMEM((parts, piece, rows), BF16),
            pltpu.VMEM((depth, rows), BF16),
            dma((chunks, n, 3)), dma((chunks, n, 3)), dma((chunks, n, 3)), dma((chunks, 3)),
            dma((9,)), dma((9,)), dma((chunks,)), dma((chunks,)),
            dma((chunks,)), dma((chunks,)), dma((chunks, 2)), dma((chunks,)),
            dma((2, 2)), dma((2, 2)), dma((2, parts)), dma((2, parts)),
            dma((parts,)), dma((parts,)), dma((6, parts)), dma((6, parts)),
            dma((2, parts)), dma((2, parts)),
        ],
        compiler_params=pltpu.CompilerParams(
            collective_id=0, has_side_effects=True, vmem_limit_bytes=56 * 2**20),
    )(tokens.T, cotangent.T, gate_weight, up_weight, down_weight.T)
    return dx.T, dg.T


def solution(mesh):
    n, tp = mesh.shape["fs"], mesh.shape["tp"]

    def per_device(tokens, cotangent, gate_weight, up_weight, down_weight):
        rows, depth = tokens.shape
        shard, ff = gate_weight.shape
        args = (tokens, cotangent, gate_weight, up_weight, down_weight)
        fits = (tp == 8 and n == 4 and rows % (2 * LANES) == 0 and rows <= 512
                and depth == n * shard and shard % SUB == 0 and ff % LANES == 0 and ff <= 512)
        return per_device_kernel(n, *args) if fits else per_device_plain(*args)

    placed = (P("fs", None), P("fs", None), P("fs", "tp"), P("fs", "tp"), P("tp", "fs"))
    return jax.shard_map(
        per_device,
        mesh=mesh,
        in_specs=placed,
        out_specs=(P("fs", None), P("tp", "fs")),
        check_vma=False,
    )
```

time: 91.3 us -> 69.9 us (0.77)
  the two profiles are of different devices: /device:TPU:0 before, /device:TPU:9 now
where the time goes in v1:
time: 69.9 us; the launch traced here: 69.8 us
  Pallas kernels  66.3 us (95%)
  local copies, waits for them, and re-layouts  2.84 us (4%)
    pallas_call x1, Pallas kernels, per_device_kernel(): pl.pallas_call(functools.partial(kernel, n), out_shape=(jax.ShapeDtypeStr...  66.3 us
    unnamed x4, local copies, waits for them, and re-layouts  2.84 us

profile of v1, /device:TPU:9, one launch (start us, length us, event | category | flops | bytes accessed | tf_op | source)
XLA Modules:
  0.0 69.8 jit_solution(17106995529423971293)
XLA Ops:
  0.6 66.3 %shard_map.68 = (bf16[1344,256]{1,0:T(8,128)(2,1)}, f32[336,384]{1,0:T(8,128)}) custom-call(bf16[1344,256]{1,0:T(8,128)(2,1)} %bitcast.5, bf16[1344,256]{1,0:T(8,128)(2,1)} %bitcast.6, bf16[336,384]{1,0:T(8,128)(2,1)} %gate_ref.1, bf16[336,384]{1,0:T(8,128)(2,1)} %up_ref.1, bf16[336,384]{1,0:T(8,128)(2,1)} %bitcast.9), custom_call_target="tpu_custom_call" | custom-call | tf_op jit(solution)/shard_map/pallas_call | solution.py:451
  66.9 0.0 copy-start
  66.9 2.0 %copy.9 = bf16[256,1344]{0,1:T(8,128)(2,1)} copy(bf16[256,1344]{0,1:T(8,128)(2,1)} %bitcast.7) | data formatting | bytes 1376256
  69.0 0.0 copy-done
  69.0 0.8 %copy.10 = f32[384,336]{0,1:T(8,128)} copy(f32[384,336]{0,1:T(8,128)S(1)} %bitcast.8) | data formatting | bytes 1032192
Async XLA Ops:
  66.9 2.1 %copy-start = (f32[336,384]{1,0:T(8,128)S(1)}, f32[336,384]{1,0:T(8,128)}, u32[]{:S(2)}) copy-start(f32[336,384]{1,0:T(8,128)} %get-tuple-element.5) | copy-start | bytes 1548292

commit v2 on v1

--- a/solution.py
+++ b/solution.py
@@ -53,12 +53,12 @@
     return (input_grad, down_grad)
 
 
-def kernel(n, tok_ref, cot_ref, gate_ref, up_ref, down_ref, dx_out, dg_out,
-           weights, tok, cot, ptok, pcot, dxacc, hid, dgp, dgs, dgr, dgf,
+def kernel(n, tok_hbm, cot_hbm, gate_hbm, up_hbm, down_hbm, dx_out, dg_out,
+           tok_ref, cot_ref, gate_ref, up_ref, down_ref, dgacc, weights, tok, cot, ptok, pcot, dxacc, hid, dgp, dgs, dgr, dgf,
            t1s, t1r, t2s, t2r, t3s, t3r, ybuf,
            z_send, s_send, w_recv, loc_sem, tk_send, tk_recv, hid_send, hid_recv,
            dg_send, dg_recv, dgf_send, dgf_recv, t1_send, t1_recv, t2_send, t2_recv,
-           t3_send, t3_recv, y_send, y_recv, yd_send, yd_recv):
+           t3_send, t3_recv, y_send, y_recv, yd_send, yd_recv, in_sem, out_sem):
     z = lax.axis_index("fs")
     b = lax.axis_index("tp")
     depth, rows = tok_ref.shape
@@ -89,6 +89,11 @@
     col_y = 2 * (1 - cy) + cx
     col_d = 2 * (1 - cy) + 1 - cx
 
+    loads = [pltpu.make_async_copy(src, dst, in_sem.at[i]) for i, (src, dst) in enumerate((
+        (tok_hbm, tok_ref), (cot_hbm, cot_ref), (gate_hbm, gate_ref), (up_hbm, up_ref),
+        (down_hbm, down_ref)))]
+    for load in loads:
+        load.start()
     barrier = pltpu.get_barrier_semaphore()
 
     def greet(fs, tp):
@@ -102,6 +107,8 @@
         greet(lax.rem(z + step, n), b)
         greet(lax.rem(z + step, n), sib)
     pl.semaphore_wait(barrier, 3 + 2 * (n - 1))
+    for load in loads:
+        load.wait()
 
     def remote(src, dst, send, recv, fs, tp):
         return pltpu.make_async_remote_copy(
@@ -221,7 +228,7 @@
 
             @pl.when(jnp.logical_and(home, zodd == i))
             def _():
-                dg_out[:, lanes_of(c)] = value
+                dgacc[:, lanes_of(c)] = value
 
             @pl.when(jnp.logical_and(home, zodd != i))
             def _():
@@ -255,12 +262,12 @@
         @pl.when(home)
         def _():
             dg_home(c).wait_recv()
-            dg_out[:, lanes_of(c)] += dgr[c, 0].astype(F32)
+            dgacc[:, lanes_of(c)] += dgr[c, 0].astype(F32)
 
         @pl.when(away)
         def _():
             dg_far(c, 0).wait_recv()
-            dg_out[:, lanes_of(c)] = dgf[c].astype(F32)
+            dgacc[:, lanes_of(c)] = dgf[c].astype(F32)
 
     low, high = slice(0, half_rows), slice(half_rows, rows)
     halves = (low, high)
@@ -286,6 +293,12 @@
     def y_half(i, k, q, tp):
         ref = ybuf.at[strip(k, q), pl.ds(i * half_rows, half_rows)]
         return remote(ref, ref, yd_send.at[i, q], yd_recv.at[i, q], z, tp)
+
+    def put(i, k, q):
+        r = strip(k, q)
+        return pltpu.make_async_copy(ybuf.at[r], dx_out.at[r], out_sem.at[i, q])
+
+    dg_put = pltpu.make_async_copy(dgacc, dg_out, out_sem.at[4, 0])
 
     def y_sib(i, k, q):
         ref = ybuf.at[strip(k, q)]
@@ -309,14 +322,14 @@
             dxacc[...] = contract_cols(w, dgu)
         elif c < chunks - 1:
             dxacc[...] += contract_cols(w, dgu)
-        if c == 0:
-            @pl.when(home)
-            def _():
-                give.wait_recv()
-        if c < chunks - 1:
-            down_part(c)
-        if 0 < c < chunks - 1:
-            down_mid(c - 1)
+        if c:
+            @pl.when(end)
+            def _():
+                if c == 1:
+                    @pl.when(home)
+                    def _():
+                        give.wait_recv()
+                down_part(c - 1)
         if c == chunks - 1:
             for k, sends in ((col_d, ((0, 0), (1, 0))), (col_x, ((0, 1),)), (col_y, ((1, 1),)), (col, ())):
                 r = rows_of(k)
@@ -329,7 +342,21 @@
                     t1s[i, step] = value[:, halves[i]].astype(BF16)
                     t1_copy(i, step).start()
 
-    down_part(chunks - 1)
+    @pl.when(end)
+    def _():
+        if chunks == 1:
+            @pl.when(home)
+            def _():
+                give.wait_recv()
+        down_part(chunks - 1)
+
+    @pl.when(near)
+    def _():
+        @pl.when(home)
+        def _():
+            give.wait_recv()
+        for c in range(chunks):
+            down_part(c)
     t1_copy(0, 0).wait_recv()
     t1_copy(1, 0).wait_recv()
     for q in range(parts):
@@ -352,7 +379,7 @@
         def _():
             t3s[q] = dxacc[strip(col, q), :].astype(BF16)
             t3_copy(q).start()
-    for c in range(max(0, chunks - 2), chunks):
+    for c in range(chunks):
         down_mid(c)
 
     @pl.when(home)
@@ -363,27 +390,32 @@
             y_copy(0, col, q, bx).start()
             y_copy(1, col, q, by).start()
             y_sib(0, col, q).start()
+            put(0, col, q).start()
         for q in range(parts):
             y_copy(0, col_x, q, bx).wait_recv()
             y_half(0, col_x, q, by).start()
             y_sib(1, col_x, q).start()
+            put(1, col_x, q).start()
             y_copy(1, col_y, q, by).wait_recv()
             y_half(1, col_y, q, bx).start()
             y_sib(2, col_y, q).start()
+            put(2, col_y, q).start()
         for q in range(parts):
             y_half(0, col_d, q, by).wait_recv()
             y_half(1, col_d, q, bx).wait_recv()
             y_sib(3, col_d, q).start()
+            put(3, col_d, q).start()
 
     for c in range(chunks):
         down_final(c)
+    dg_put.start()
 
     @pl.when(away)
     def _():
         for q in range(parts):
             for i, k in enumerate((col, col_x, col_y, col_d)):
                 y_sib(i, k, q).wait_recv()
-    dx_out[...] = ybuf[...]
+                put(i, k, q).start()
 
     @pl.when(home)
     def _():
@@ -431,6 +463,10 @@
                 for i in range(2):
                     dg_far(c, i).wait_send()
 
+    for q in range(parts):
+        for i, k in enumerate((col, col_x, col_y, col_d)):
+            put(i, k, q).wait()
+    dg_put.wait()
     for c in range(chunks):
         hid_copy(c).wait_send()
     for i in range(2):
@@ -450,11 +486,16 @@
     dma = pltpu.SemaphoreType.DMA
     dx, dg = pl.pallas_call(
         functools.partial(kernel, n),
-        out_shape=(jax.ShapeDtypeStruct((depth, rows), BF16),
-                   jax.ShapeDtypeStruct((shard, ff), F32)),
-        in_specs=[vmem] * 5,
-        out_specs=(vmem, vmem),
+        out_shape=(pltpu.VMEM((depth, rows), BF16), pltpu.VMEM((shard, ff), F32)),
+        in_specs=[pl.BlockSpec(memory_space=pltpu.HBM)] * 5,
+        out_specs=[pl.BlockSpec(memory_space=pl.ANY)] * 2,
         scratch_shapes=[
+            pltpu.VMEM((depth, rows), BF16),
+            pltpu.VMEM((depth, rows), BF16),
+            pltpu.VMEM((shard, ff), BF16),
+            pltpu.VMEM((shard, ff), BF16),
+            pltpu.VMEM((shard, ff), BF16),
+            pltpu.VMEM((shard, ff), F32),
             pltpu.VMEM((depth, 3 * ff), BF16),
             pltpu.VMEM((rows, depth), BF16),
             pltpu.VMEM((rows, depth), BF16),
@@ -478,11 +519,12 @@
             dma((chunks,)), dma((chunks,)), dma((chunks, 2)), dma((chunks,)),
             dma((2, 2)), dma((2, 2)), dma((2, parts)), dma((2, parts)),
             dma((parts,)), dma((parts,)), dma((6, parts)), dma((6, parts)),
-            dma((2, parts)), dma((2, parts)),
+            dma((2, parts)), dma((2, parts)), dma((5,)), dma((5, parts)),
         ],
         compiler_params=pltpu.CompilerParams(
-            collective_id=0, has_side_effects=True, vmem_limit_bytes=56 * 2**20),
-    )(tokens.T, cotangent.T, gate_weight, up_weight, down_weight.T)
+            collective_id=0, has_side_effects=True, vmem_limit_bytes=28 * 2**20),
+    )(*(pltpu.with_memory_space_constraint(a, pltpu.HBM) for a in (
+        tokens.T, cotangent.T, gate_weight, up_weight, down_weight.T)))
     return dx.T, dg.T
 
 

time: 69.9 us -> 63.4 us (0.907)
  Pallas kernels: 66.3 us -> 61 us
  local copies, waits for them, and re-layouts: 2.84 us -> 1.64 us
    pallas_call x1, Pallas kernels: 66.3 us -> 61 us  [per_device_kernel(): pl.pallas_call(functools.partial(kernel, n), out_shape=(pltpu.VMEM((depth...]
    unnamed x4 -> x2, local copies, waits for them, and re-layouts: 2.84 us -> 1.64 us
where the time goes in v2:
time: 63.4 us; the launch traced here: 63.2 us
  Pallas kernels  61 us (96%)
  local copies, waits for them, and re-layouts  1.64 us (3%)
  between operations  0.64 us (1%)
    pallas_call x1, Pallas kernels, per_device_kernel(): pl.pallas_call(functools.partial(kernel, n), out_shape=(pltpu.VMEM((depth...  61 us
    unnamed x2, local copies, waits for them, and re-layouts  1.64 us

profile of v2, /device:TPU:9, one launch (start us, length us, event | category | flops | bytes accessed | tf_op | source)
XLA Modules:
  0.0 63.2 jit_solution(10361476980521410787)
XLA Ops:
  0.6 61.0 %shard_map.68 = (bf16[1344,256]{1,0:T(8,128)(2,1)S(1)}, f32[336,384]{1,0:T(8,128)S(1)}) custom-call(bf16[1344,256]{1,0:T(8,128)(2,1)} %bitcast.7, bf16[1344,256]{1,0:T(8,128)(2,1)} %bitcast.8, bf16[336,384]{1,0:T(8,128)(2,1)} %gate_hbm.1, bf16[336,384]{1,0:T(8,128)(2,1)} %up_hbm.1, bf16[336,384]{1,0:T(8,128)(2,1)} %bitcast.9), custom_call_target="tpu_custom_call" | custom-call | tf_op jit(solution)/shard_map/pallas_call | solution.py:487
  61.6 0.8 %copy.9 = bf16[256,1344]{0,1:T(8,128)(2,1)} copy(bf16[256,1344]{0,1:T(8,128)(2,1)S(1)} %bitcast.5) | data formatting | bytes 1376256
  62.5 0.8 %copy.10 = f32[384,336]{0,1:T(8,128)} copy(f32[384,336]{0,1:T(8,128)S(1)} %bitcast.6) | data formatting | bytes 1032192

commit v3 on v2

--- a/solution.py
+++ b/solution.py
@@ -55,10 +55,9 @@
 
 def kernel(n, tok_hbm, cot_hbm, gate_hbm, up_hbm, down_hbm, dx_out, dg_out,
            tok_ref, cot_ref, gate_ref, up_ref, down_ref, dgacc, weights, tok, cot, ptok, pcot, dxacc, hid, dgp, dgs, dgr, dgf,
-           t1s, t1r, t2s, t2r, t3s, t3r, ybuf,
-           z_send, s_send, w_recv, loc_sem, tk_send, tk_recv, hid_send, hid_recv,
-           dg_send, dg_recv, dgf_send, dgf_recv, t1_send, t1_recv, t2_send, t2_recv,
-           t3_send, t3_recv, y_send, y_recv, yd_send, yd_recv, in_sem, out_sem):
+           t1s, t1r, t2s, t2r, t3s, t3r, ownr, ybuf, tally,
+           sent, w_recv, tk_recv, hid_recv, dg_recv, dgf_recv, t1_recv, t2_recv,
+           t3_recv, own_recv, y_recv, local_sem):
     z = lax.axis_index("fs")
     b = lax.axis_index("tp")
     depth, rows = tok_ref.shape
@@ -80,8 +79,11 @@
     sib = b + 1 - 2 * core
     bx = b + 2 * (1 - 2 * cx)
     by = b + 4 * (1 - 2 * cy)
+    bd = bx + by - b
+    last = 2 * col + 1
+    lead = core == 1
     zs = z + 1 - 2 * zodd
-    zp = lax.rem(z + 2, 4)
+    zp = 3 - z
     zn = 2 - side
     zf = 3 - 3 * side
     me = jnp.where(home, 0, 1)
@@ -89,11 +91,13 @@
     col_y = 2 * (1 - cy) + cx
     col_d = 2 * (1 - cy) + 1 - cx
 
-    loads = [pltpu.make_async_copy(src, dst, in_sem.at[i]) for i, (src, dst) in enumerate((
-        (tok_hbm, tok_ref), (cot_hbm, cot_ref), (gate_hbm, gate_ref), (up_hbm, up_ref),
-        (down_hbm, down_ref)))]
-    for load in loads:
-        load.start()
+    for src, dst, i in ((tok_hbm, tok_ref, 0), (cot_hbm, cot_ref, 0), (gate_hbm, gate_ref, 1),
+                        (up_hbm, up_ref, 1), (down_hbm, down_ref, 1)):
+        pltpu.make_async_copy(src, dst, local_sem.at[i]).start()
+
+    def drain(ref, sem):
+        pltpu.make_async_copy(ref, ref, sem).wait()
+
     barrier = pltpu.get_barrier_semaphore()
 
     def greet(fs, tp):
@@ -103,12 +107,13 @@
     greet(z, sib)
     greet(z, bx)
     greet(z, by)
+    greet(z, bd)
     for step in range(1, n):
         greet(lax.rem(z + step, n), b)
         greet(lax.rem(z + step, n), sib)
-    pl.semaphore_wait(barrier, 3 + 2 * (n - 1))
-    for load in loads:
-        load.wait()
+    pl.semaphore_wait(barrier, 4 + 2 * (n - 1))
+    drain(tally.at[pl.ds(0, 2 * depth)], local_sem.at[0])
+    drain(weights.at[pl.ds(0, shard)], local_sem.at[1])
 
     def remote(src, dst, send, recv, fs, tp):
         return pltpu.make_async_remote_copy(
@@ -124,21 +129,21 @@
     def own(c, kind):
         return (gate_ref, up_ref, down_ref)[kind].at[:, pl.ds(c * LANES, LANES)]
 
-    def w_copy(src, c, k, kind, fs):
-        return remote(src, slot(c, k, kind), z_send.at[c, k, kind], w_recv.at[c, k, kind], fs, b)
+    def w_copy(src, c, k, kind, i, fs):
+        return remote(src, slot(c, k, kind), sent.at[0], w_recv.at[c, i, kind], fs, b)
 
     def sib_copy(src, c, k, kind):
-        return remote(src, slot(c, k, kind), s_send.at[c, k, kind], w_recv.at[c, k, kind], z, sib)
+        return remote(src, slot(c, k, kind), sent.at[1], w_recv.at[c, 0, 0], z, sib)
 
     def local_copy(c, kind):
-        return pltpu.make_async_copy(own(c, kind), slot(c, z, kind), loc_sem.at[c, kind])
+        return pltpu.make_async_copy(own(c, kind), slot(c, z, kind), local_sem.at[2])
 
     every = [(c, kind) for c in range(chunks) for kind in range(3)]
     mine_q = rows_of(col)
     far_rows = rows_of(2 * side, 2)
 
     def tk_copy(i, src, dst, fs, tp):
-        return remote(src, dst, tk_send.at[i], tk_recv.at[i], fs, tp)
+        return remote(src, dst, sent.at[2], tk_recv.at[i], fs, tp)
 
     tok_hop = tk_copy(0, tok_ref.at[mine_q], ptok.at[mine_q], zp, b)
     cot_hop = tk_copy(1, cot_ref.at[mine_q], pcot.at[mine_q], zp, sib)
@@ -150,9 +155,9 @@
 
     @pl.when(home)
     def _():
-        remote(tok_ref.at[mine_q], ptok.at[mine_q], tk_send.at[0], tk_recv.at[0], zp, b).start()
+        tok_hop.start()
         for c, kind in every:
-            w_copy(own(c, kind), c, z, kind, zs).start()
+            w_copy(own(c, kind), c, z, kind, 0, zs).start()
             sib_copy(own(c, kind), c, z, kind).start()
             local_copy(c, kind).start()
         tok[...] = tok_ref[...].T
@@ -160,9 +165,9 @@
 
     @pl.when(away)
     def _():
-        remote(cot_ref.at[mine_q], pcot.at[mine_q], tk_send.at[1], tk_recv.at[1], zp, sib).start()
+        cot_hop.start()
         for c, kind in every:
-            w_copy(own(c, kind), c, z, kind, zn).start()
+            w_copy(own(c, kind), c, z, kind, jnp.where(near, 1, 2), zn).start()
         tok_hop.wait_recv()
         spread(2, ptok, col, bx).start()
         spread(3, ptok, col, by).start()
@@ -188,32 +193,30 @@
         def _():
             for kind in range(3):
                 for i, k in enumerate(others):
-                    w_copy(slot(c, k, kind), c, k, kind, zs).wait_recv()
+                    w_copy(slot(c, k, kind), c, k, kind, i, zs).wait_recv()
                     if i:
                         @pl.when(near)
                         def _():
-                            w_copy(slot(c, k, kind), c, k, kind, zs).start()
+                            w_copy(slot(c, k, kind), c, k, kind, i, zs).start()
                     sib_copy(slot(c, k, kind), c, k, kind).start()
-            for kind in range(3):
-                local_copy(c, kind).wait()
+            if c == 0:
+                drain(weights.at[rows_of(z)], local_sem.at[2])
 
         @pl.when(away)
         def _():
-            for kind in range(3):
-                for k in range(n):
-                    sib_copy(slot(c, k, kind), c, k, kind).wait_recv()
+            drain(weights.at[:, pl.ds(3 * c * LANES, 3 * LANES)], w_recv.at[c, 0, 0])
 
     def hid_copy(c):
-        return remote(hid.at[me, c], hid.at[me, c], hid_send.at[c], hid_recv.at[c], z, sib)
+        return remote(hid.at[me, c], hid.at[me, c], sent.at[3], hid_recv.at[c], z, sib)
 
     def dg_home(c):
-        return remote(dgs.at[c, 0], dgr.at[c, 0], dg_send.at[c], dg_recv.at[c], zs, b)
+        return remote(dgs.at[c, 0], dgr.at[c, 0], sent.at[4], dg_recv.at[c], zs, b)
 
     def dg_away(c):
-        return remote(dgs.at[c], dgr.at[c], dg_send.at[c], dg_recv.at[c], zs, b)
+        return remote(dgs.at[c], dgr.at[c], sent.at[4], dg_recv.at[c], zs, b)
 
     def dg_far(c, i):
-        return remote(dgs.at[c, i], dgf.at[c], dgf_send.at[c, i], dgf_recv.at[c],
+        return remote(dgs.at[c, i], dgf.at[c], sent.at[4], dgf_recv.at[c],
                       2 * (1 - side) + i, sib)
 
     def lanes_of(c):
@@ -273,36 +276,35 @@
     halves = (low, high)
 
     def t1_copy(i, step):
-        return remote(t1s.at[i, step], t1r.at[i, step], t1_send.at[i, step], t1_recv.at[i, step],
+        return remote(t1s.at[i, step], t1r.at[i, step], sent.at[5], t1_recv.at[i, step],
                       z, bx if i == 0 else by)
 
     def t2_copy(i, q):
-        return remote(t2s.at[i, q], t2r.at[i, q], t2_send.at[i, q], t2_recv.at[i, q],
+        return remote(t2s.at[i, q], t2r.at[i, q], sent.at[6], t2_recv.at[i, q],
                       z, by if i == 0 else bx)
 
     def t3_copy(q):
-        return remote(t3s.at[q], t3r.at[q], t3_send.at[q], t3_recv.at[q], zp, b)
+        return remote(t3s.at[q], t3r.at[q], sent.at[7], t3_recv.at[q], zp, last)
 
     def strip(k, q):
         return pl.ds(pl.multiple_of(k * shard + q * piece, SUB), piece)
 
+    def own_copy(q):
+        return remote(dxacc.at[strip(col, q)], ownr.at[q], sent.at[7], own_recv.at[q], z, sib)
+
     def y_copy(i, k, q, tp):
         ref = ybuf.at[strip(k, q)]
-        return remote(ref, ref, y_send.at[i, q], y_recv.at[i, q], z, tp)
-
-    def y_half(i, k, q, tp):
-        ref = ybuf.at[strip(k, q), pl.ds(i * half_rows, half_rows)]
-        return remote(ref, ref, yd_send.at[i, q], yd_recv.at[i, q], z, tp)
-
-    def put(i, k, q):
-        r = strip(k, q)
-        return pltpu.make_async_copy(ybuf.at[r], dx_out.at[r], out_sem.at[i, q])
-
-    dg_put = pltpu.make_async_copy(dgacc, dg_out, out_sem.at[4, 0])
+        return remote(ref, ref, sent.at[8], y_recv.at[i, q], z, tp)
 
     def y_sib(i, k, q):
         ref = ybuf.at[strip(k, q)]
-        return remote(ref, ref, y_send.at[2 + i, q], y_recv.at[2 + i, q], z, sib)
+        return remote(ref, ref, sent.at[9], y_recv.at[i, q], z, sib)
+
+    def put(k, q):
+        r = strip(k, q)
+        return pltpu.make_async_copy(ybuf.at[r], dx_out.at[r], local_sem.at[3])
+
+    dg_put = pltpu.make_async_copy(dgacc, dg_out, local_sem.at[4])
 
     for c in range(chunks):
         gather(c)
@@ -379,101 +381,87 @@
         def _():
             t3s[q] = dxacc[strip(col, q), :].astype(BF16)
             t3_copy(q).start()
+
+        @pl.when(jnp.logical_and(home, core == 0))
+        def _():
+            own_copy(q).start()
+
     for c in range(chunks):
         down_mid(c)
 
-    @pl.when(home)
+    places = (col, col_x, col_y, col_d)
+
+    @pl.when(lead)
     def _():
         for q in range(parts):
             t3_copy(q).wait_recv()
-            ybuf[strip(col, q), :] = (dxacc[strip(col, q), :] + t3r[q].astype(F32)).astype(BF16)
+
+            @pl.when(home)
+            def _():
+                ybuf[strip(col, q), :] = (dxacc[strip(col, q), :] + t3r[q].astype(F32)).astype(BF16)
+
+            @pl.when(away)
+            def _():
+                own_copy(q).wait_recv()
+                ybuf[strip(col, q), :] = (ownr[q] + t3r[q].astype(F32)).astype(BF16)
+
+            y_copy(2, col, q, bd).start()
             y_copy(0, col, q, bx).start()
             y_copy(1, col, q, by).start()
             y_sib(0, col, q).start()
-            put(0, col, q).start()
+            put(col, q).start()
         for q in range(parts):
-            y_copy(0, col_x, q, bx).wait_recv()
-            y_half(0, col_x, q, by).start()
-            y_sib(1, col_x, q).start()
-            put(1, col_x, q).start()
-            y_copy(1, col_y, q, by).wait_recv()
-            y_half(1, col_y, q, bx).start()
-            y_sib(2, col_y, q).start()
-            put(2, col_y, q).start()
-        for q in range(parts):
-            y_half(0, col_d, q, by).wait_recv()
-            y_half(1, col_d, q, bx).wait_recv()
-            y_sib(3, col_d, q).start()
-            put(3, col_d, q).start()
+            for i, k, tp in ((0, col_x, bx), (1, col_y, by), (2, col_d, bd)):
+                y_copy(i, k, q, tp).wait_recv()
+                y_sib(i + 1, k, q).start()
+                put(k, q).start()
 
     for c in range(chunks):
         down_final(c)
     dg_put.start()
 
+    @pl.when(core == 0)
+    def _():
+        for q in range(parts):
+            for i, k in enumerate(places):
+                y_sib(i, k, q).wait_recv()
+                put(k, q).start()
+
+    @pl.when(lead)
+    def _():
+        drain(ybuf.at[pl.ds(0, 3 * shard)], sent.at[8])
+        drain(ybuf, sent.at[9])
+
+    @pl.when(home)
+    def _():
+        drain(ybuf.at[pl.ds(0, shard)], sent.at[2])
+        drain(weights, sent.at[1])
+        drain(dgs.at[:, 0], sent.at[4])
+
+        @pl.when(near)
+        def _():
+            drain(weights.at[pl.ds(0, 3 * shard)], sent.at[0])
+
+        @pl.when(end)
+        def _():
+            drain(weights.at[pl.ds(0, shard)], sent.at[0])
+
+        @pl.when(core == 0)
+        def _():
+            drain(ownr, sent.at[7])
+
     @pl.when(away)
     def _():
-        for q in range(parts):
-            for i, k in enumerate((col, col_x, col_y, col_d)):
-                y_sib(i, k, q).wait_recv()
-                put(i, k, q).start()
-
-    @pl.when(home)
-    def _():
-        tok_hop.wait_send()
-        for c, kind in every:
-            w_copy(own(c, kind), c, z, kind, zs).wait_send()
-            sib_copy(own(c, kind), c, z, kind).wait_send()
-            for i, k in enumerate(others):
-                sib_copy(slot(c, k, kind), c, k, kind).wait_send()
-                if i:
-                    @pl.when(near)
-                    def _():
-                        w_copy(slot(c, k, kind), c, k, kind, zs).wait_send()
-        for c in range(chunks):
-            dg_home(c).wait_send()
-        for q in range(parts):
-            y_copy(0, col, q, bx).wait_send()
-            y_copy(1, col, q, by).wait_send()
-            y_half(0, col_x, q, by).wait_send()
-            y_half(1, col_y, q, bx).wait_send()
-            for i, k in enumerate((col, col_x, col_y, col_d)):
-                y_sib(i, k, q).wait_send()
-
-    @pl.when(away)
-    def _():
-        cot_hop.wait_send()
-        for c, kind in every:
-            w_copy(own(c, kind), c, z, kind, zn).wait_send()
-        spread(2, ptok, col, bx).wait_send()
-        spread(3, ptok, col, by).wait_send()
-        spread(4, pcot, col, bx).wait_send()
-        spread(5, pcot, col, by).wait_send()
-        spread(6, ptok, col_x, by).wait_send()
-        spread(7, pcot, col_y, bx).wait_send()
-        give.wait_send()
-        for q in range(parts):
-            t3_copy(q).wait_send()
-        for c in range(chunks):
-            @pl.when(end)
-            def _():
-                dg_away(c).wait_send()
-
-            @pl.when(near)
-            def _():
-                for i in range(2):
-                    dg_far(c, i).wait_send()
-
-    for q in range(parts):
-        for i, k in enumerate((col, col_x, col_y, col_d)):
-            put(i, k, q).wait()
+        drain(weights.at[pl.ds(0, shard)], sent.at[0])
+        drain(tally, sent.at[2])
+        drain(dgs, sent.at[4])
+        drain(t3s, sent.at[7])
+
+    drain(hid.at[0], sent.at[3])
+    drain(t1s, sent.at[5])
+    drain(t2s, sent.at[6])
+    drain(ybuf, local_sem.at[3])
     dg_put.wait()
-    for c in range(chunks):
-        hid_copy(c).wait_send()
-    for i in range(2):
-        for step in range(2):
-            t1_copy(i, step).wait_send()
-        for q in range(parts):
-            t2_copy(i, q).wait_send()
 
 
 def per_device_kernel(n, tokens, cotangent, gate_weight, up_weight, down_weight):
@@ -513,13 +501,12 @@
             pltpu.VMEM((2, parts, piece, rows // 2), BF16),
             pltpu.VMEM((parts, piece, rows), BF16),
             pltpu.VMEM((parts, piece, rows), BF16),
+            pltpu.VMEM((parts, piece, rows), F32),
             pltpu.VMEM((depth, rows), BF16),
-            dma((chunks, n, 3)), dma((chunks, n, 3)), dma((chunks, n, 3)), dma((chunks, 3)),
-            dma((9,)), dma((9,)), dma((chunks,)), dma((chunks,)),
-            dma((chunks,)), dma((chunks,)), dma((chunks, 2)), dma((chunks,)),
-            dma((2, 2)), dma((2, 2)), dma((2, parts)), dma((2, parts)),
-            dma((parts,)), dma((parts,)), dma((6, parts)), dma((6, parts)),
-            dma((2, parts)), dma((2, parts)), dma((5,)), dma((5, parts)),
+            pltpu.VMEM((9 * shard, rows), BF16),
+            dma((10,)), dma((chunks, 3, 3)), dma((9,)), dma((chunks,)), dma((chunks,)),
+            dma((chunks,)), dma((2, 2)), dma((2, parts)), dma((parts,)), dma((parts,)),
+            dma((4, parts)), dma((5,)),
         ],
         compiler_params=pltpu.CompilerParams(
             collective_id=0, has_side_effects=True, vmem_limit_bytes=28 * 2**20),

time: 63.4 us -> 61.3 us (0.967)
  the two profiles are of different devices: /device:TPU:9 before, /device:TPU:0 now
where the time goes in v3:
time: 61.3 us; the launch traced here: 61.2 us
  Pallas kernels  58.9 us (96%)
  local copies, waits for them, and re-layouts  1.64 us (3%)
  between operations  0.64 us (1%)
    pallas_call x1, Pallas kernels, per_device_kernel(): pl.pallas_call(functools.partial(kernel, n), out_shape=(pltpu.VMEM((depth...  58.9 us
    unnamed x2, local copies, waits for them, and re-layouts  1.64 us

profile of v3, /device:TPU:0, one launch (start us, length us, event | category | flops | bytes accessed | tf_op | source)
XLA Modules:
  0.0 61.2 jit_solution(3375736788056276924)
XLA Ops:
  0.6 58.9 %shard_map.68 = (bf16[1344,256]{1,0:T(8,128)(2,1)S(1)}, f32[336,384]{1,0:T(8,128)S(1)}) custom-call(bf16[1344,256]{1,0:T(8,128)(2,1)} %bitcast.7, bf16[1344,256]{1,0:T(8,128)(2,1)} %bitcast.8, bf16[336,384]{1,0:T(8,128)(2,1)} %gate_hbm.1, bf16[336,384]{1,0:T(8,128)(2,1)} %up_hbm.1, bf16[336,384]{1,0:T(8,128)(2,1)} %bitcast.9), custom_call_target="tpu_custom_call" | custom-call | tf_op jit(solution)/shard_map/pallas_call | solution.py:475
  59.6 0.8 %copy.9 = bf16[256,1344]{0,1:T(8,128)(2,1)} copy(bf16[256,1344]{0,1:T(8,128)(2,1)S(1)} %bitcast.5) | data formatting | bytes 1376256
  60.4 0.8 %copy.10 = f32[384,336]{0,1:T(8,128)} copy(f32[384,336]{0,1:T(8,128)S(1)} %bitcast.6) | data formatting | bytes 1032192

commit v4 on v3

v4 whole, which is shorter than its diff:
```python
import functools

import jax
import jax.numpy as jnp
from jax import lax
from jax.experimental import pallas as pl
from jax.experimental.pallas import tpu as pltpu
from jax.sharding import PartitionSpec as P

LANES = 128
SUB = 16
BF16 = jnp.bfloat16
F32 = jnp.float32


def contract_rows(left, right):
    return lax.dot_general(
        left, right, (((0,), (0,)), ((), ())), preferred_element_type=jnp.float32
    )


def contract_cols(left, right):
    return lax.dot_general(
        left, right, (((1,), (1,)), ((), ())), preferred_element_type=jnp.float32
    )


def send_down(hidden, cotangent):
    return lax.psum_scatter(
        contract_rows(cotangent, hidden), "fs", scatter_dimension=0, tiled=True
    ).T


def per_device_plain(tokens, cotangent, gate_weight, up_weight, down_weight):
    whole_gate, whole_up, whole_down = (
        lax.all_gather(gate_weight, "fs", axis=0, tiled=True),
        lax.all_gather(up_weight, "fs", axis=0, tiled=True),
        lax.all_gather(down_weight, "fs", axis=1, tiled=True),
    )
    gate_pre = jnp.dot(tokens, whole_gate, preferred_element_type=jnp.float32)
    up_pre = jnp.dot(tokens, whole_up, preferred_element_type=jnp.float32)
    hidden_grad = contract_cols(cotangent, whole_down)
    sigmoid_gate = jax.nn.sigmoid(gate_pre)
    activated = gate_pre * sigmoid_gate
    hidden = (activated * up_pre).astype(jnp.bfloat16)
    gate_pre_grad = (
        hidden_grad * up_pre * sigmoid_gate * (1.0 + gate_pre * (1.0 - sigmoid_gate))
    ).astype(jnp.bfloat16)
    up_pre_grad = (hidden_grad * activated).astype(jnp.bfloat16)
    partial_value = contract_cols(gate_pre_grad, whole_gate) + contract_cols(up_pre_grad, whole_up)
    input_grad = lax.psum(partial_value.astype(jnp.bfloat16), "tp")
    down_grad = send_down(hidden, cotangent)
    return (input_grad, down_grad)


def kernel(n, tok_hbm, cot_hbm, gate_hbm, up_hbm, down_hbm, dx_out, dg_out,
           tok_ref, cot_ref, gate_ref, up_ref, down_ref, weights, tok, cot,
           ptok, pcot, etok, ecot, dxacc, hid, dgacc, dgs, dgr,
           t1s, t1r, t2s, t2r, t3s, t3r, ownr, ybuf, tally,
           sent, w_recv, tk_recv, hid_recv, dg_recv, t1_recv, t2_recv,
           t3_recv, own_recv, y_recv, local_sem):
    z = lax.axis_index("fs")
    b = lax.axis_index("tp")
    depth, rows = tok_ref.shape
    shard, ff = gate_ref.shape
    chunks = ff // LANES
    parts, piece = t2s.shape[2], t2s.shape[3]
    half_rows = rows // 2
    core = lax.rem(b, 2)
    col = lax.div(b, 2)
    cx = lax.rem(col, 2)
    cy = lax.div(col, 2)
    side = lax.div(z, 2)
    zodd = lax.rem(z, 2)
    home = core == side
    away = core != side
    near = side != zodd
    end = side == zodd
    lead = core == 1
    sib = b + 1 - 2 * core
    bx = b + 2 * (1 - 2 * cx)
    by = b + 4 * (1 - 2 * cy)
    bd = bx + by - b
    last = 2 * col + 1
    zs = z + 1 - 2 * zodd
    zn = 2 - side
    zf = 3 - 3 * side
    me = jnp.where(home, 0, 1)
    col_x = 2 * cy + 1 - cx
    col_y = 2 * (1 - cy) + cx
    col_d = 2 * (1 - cy) + 1 - cx
    for src, dst, i in ((tok_hbm, tok_ref, 0), (cot_hbm, cot_ref, 0), (gate_hbm, gate_ref, 1),
                        (up_hbm, up_ref, 1), (down_hbm, down_ref, 1)):
        pltpu.make_async_copy(src, dst, local_sem.at[i]).start()

    def drain(ref, sem):
        pltpu.make_async_copy(ref, ref, sem).wait()

    barrier = pltpu.get_barrier_semaphore()

    def greet(fs, tp):
        pl.semaphore_signal(barrier, inc=1, device_id={"fs": fs, "tp": tp},
                            device_id_type=pl.DeviceIdType.MESH)

    greet(z, sib)
    greet(z, bx)
    greet(z, by)
    greet(z, bd)
    for step in range(1, n):
        greet(lax.rem(z + step, n), b)
        greet(lax.rem(z + step, n), sib)
    pl.semaphore_wait(barrier, 4 + 2 * (n - 1))
    drain(tally.at[pl.ds(0, 2 * depth)], local_sem.at[0])
    drain(weights.at[pl.ds(0, shard)], local_sem.at[1])

    def remote(src, dst, send, recv, fs, tp):
        return pltpu.make_async_remote_copy(
            src_ref=src, dst_ref=dst, send_sem=send, recv_sem=recv,
            device_id={"fs": fs, "tp": tp}, device_id_type=pl.DeviceIdType.MESH)

    def rows_of(k, count=1):
        return pl.ds(pl.multiple_of(k * shard, SUB), count * shard)

    def lanes_of(c, count=1):
        return pl.ds(c * LANES, count * LANES)

    def slot(c, k, kind):
        return weights.at[rows_of(k), lanes_of(3 * c + kind)]

    def own(c, kind):
        return (gate_ref, up_ref, down_ref)[kind].at[:, lanes_of(c)]

    def w_copy(c, k, kind, i, fs):
        return remote(own(c, kind), slot(c, k, kind), sent.at[0], w_recv.at[c, i, kind], fs, b)

    def sib_copy(src, c, k, kind):
        return remote(src, slot(c, k, kind), sent.at[1], w_recv.at[c, 0, 0], z, sib)

    every = [(c, kind) for c in range(chunks) for kind in range(3)]
    others = (zs, zn, zf)
    mine_q = rows_of(col)

    def tk_copy(i, src, dst, fs, tp):
        return remote(src, dst, sent.at[2], tk_recv.at[i], fs, tp)

    def tok_buf(e):
        return etok if e else ptok

    def cot_buf(e):
        return ecot.at[me] if e else pcot

    def spread(i, e, q, tp):
        buf = cot_buf(e) if i in (1, 4, 5, 7) else tok_buf(e)
        ref = buf.at[rows_of(q)]
        return tk_copy(8 * e + i, ref, ref, z, tp)

    def spread_first(e):
        spread(0, e, col, bx).wait_recv()
        spread(2, e, col, bx).start()
        spread(3, e, col, by).start()
        spread(1, e, col, bx).wait_recv()
        spread(4, e, col, bx).start()
        spread(5, e, col, by).start()

    def spread_second(e):
        spread(2, e, col_x, bx).wait_recv()
        spread(6, e, col_x, by).start()
        spread(5, e, col_y, by).wait_recv()
        spread(7, e, col_y, bx).start()

    def spread_rest(e):
        spread(3, e, col_y, by).wait_recv()
        spread(6, e, col_d, by).wait_recv()
        spread(4, e, col_x, bx).wait_recv()
        spread(7, e, col_d, bx).wait_recv()

    far_rows = rows_of(2 * (1 - core), 2)
    give = tk_copy(16, pcot.at[far_rows], pcot.at[far_rows], z, sib)
    give_extra = tk_copy(17, ecot.at[me, far_rows], ecot.at[me, far_rows], z, sib)
    take_extra = tk_copy(17, ecot.at[1 - me, far_rows], ecot.at[1 - me, far_rows], z, sib)
    @pl.when(jnp.logical_and(end, home))
    def _():
        tk_copy(8, tok_ref.at[mine_q], etok.at[mine_q], zn, b).start()
        tk_copy(8, tok_ref.at[mine_q], etok.at[mine_q], zs, b).start()
        for c, kind in every:
            w_copy(c, z, kind, 0, zs).start()

    @pl.when(jnp.logical_and(end, away))
    def _():
        tk_copy(9, cot_ref.at[mine_q], ecot.at[1, mine_q], zn, sib).start()
        tk_copy(9, cot_ref.at[mine_q], ecot.at[0, mine_q], zs, sib).start()
        for c, kind in every:
            w_copy(c, z, kind, 2, zn).start()

    @pl.when(jnp.logical_and(near, home))
    def _():
        tk_copy(0, tok_ref.at[mine_q], ptok.at[mine_q], zn, b).start()
        for c, kind in every:
            sib_copy(own(c, kind), c, z, kind).start()
            pltpu.make_async_copy(own(c, kind), slot(c, z, kind), local_sem.at[2]).start()
        tok[0] = tok_ref[...].T
        cot[0] = cot_ref[...].T
        spread_first(1)
        spread_second(1)

    @pl.when(jnp.logical_and(near, away))
    def _():
        tk_copy(1, cot_ref.at[mine_q], pcot.at[mine_q], zn, sib).start()
        for c, kind in every:
            w_copy(c, z, kind, 1, zn).start()
        spread_first(0)
        spread_first(1)
        spread_second(0)
        spread_second(1)
        spread_rest(0)
        give.start()
        tok[0] = ptok[...].T
        cot[0] = pcot[...].T

    def gather(c):
        @pl.when(home)
        def _():
            for kind in range(3):
                for i, k in enumerate(others):
                    w_copy(c, k, kind, i, zs).wait_recv()
                    sib_copy(slot(c, k, kind), c, k, kind).start()
            if c == 0:
                drain(weights.at[rows_of(z)], local_sem.at[2])

        @pl.when(away)
        def _():
            drain(weights.at[:, lanes_of(3 * c, 3)], w_recv.at[c, 0, 0])

    def hid_copy(e, c):
        ref = hid.at[e, me, :, lanes_of(c)]
        return remote(ref, ref, sent.at[3], hid_recv.at[e, c], z, sib)

    def activate(e, c):
        pre = jnp.dot(tok[e], weights[:, 3 * c * LANES:(3 * c + 2) * LANES],
                      preferred_element_type=F32)
        hg = jnp.dot(cot[e], weights[:, (3 * c + 2) * LANES:(3 * c + 3) * LANES],
                     preferred_element_type=F32)
        gate_pre, up_pre = pre[:, :LANES], pre[:, LANES:]
        sig = jax.nn.sigmoid(gate_pre)
        act = gate_pre * sig
        hid[e, me, :, lanes_of(c)] = (act * up_pre).astype(BF16)
        hid_copy(e, c).start()
        return jnp.concatenate(
            [(hg * up_pre * sig * (1.0 + gate_pre * (1.0 - sig))).astype(BF16),
             (hg * act).astype(BF16)], axis=1)

    def work(e, c):
        dgu = activate(e, c)
        value = contract_cols(weights[:, 3 * c * LANES:(3 * c + 2) * LANES], dgu)
        if c == 0:
            dxacc[e] = value
        else:
            dxacc[e] += value

    halves = (slice(0, half_rows), slice(half_rows, rows))

    def t1_copy(e, i, step):
        return remote(t1s.at[e, i, step], t1r.at[e, i, step], sent.at[5], t1_recv.at[e, i, step],
                      z, bx if i == 0 else by)

    def t2_copy(e, i, q):
        return remote(t2s.at[e, i, q], t2r.at[e, i, q], sent.at[6], t2_recv.at[e, i, q],
                      z, by if i == 0 else bx)

    def t3_copy(e, i, q, fs):
        return remote(t3s.at[e, q], t3r.at[i, q], sent.at[7], t3_recv.at[i, q], fs, last)

    def strip(k, q):
        return pl.ds(pl.multiple_of(k * shard + q * piece, SUB), piece)

    def own_copy(q):
        return remote(dxacc.at[0, strip(col, q)], ownr.at[q], sent.at[10], own_recv.at[q], z, sib)

    def work_last(e, c, at_once):
        dgu = activate(e, c)
        for k, sends in ((col_d, ((0, 0), (1, 0))), (col_x, ((0, 1),)), (col_y, ((1, 1),)), (col, ())):
            r = rows_of(k)
            value = contract_cols(weights[r, 3 * c * LANES:(3 * c + 2) * LANES], dgu)
            if c:
                value = value + dxacc[e, r, :]
            if k is not col_d:
                dxacc[e, r, :] = value
            for i, step in sends:
                t1s[e, i, step] = value[:, halves[i]].astype(BF16)
                if at_once:
                    t1_copy(e, i, step).start()

    def second_step(e):
        t1_copy(e, 0, 0).wait_recv()
        t1_copy(e, 1, 0).wait_recv()
        for q in range(parts):
            inner = slice(q * piece, (q + 1) * piece)
            for i, k in ((0, col_y), (1, col_x)):
                t2s[e, i, q] = (dxacc[e, strip(k, q), halves[i]]
                                + t1r[e, i, 0, inner].astype(F32)).astype(BF16)
                t2_copy(e, i, q).start()

    def collect(e):
        t1_copy(e, 0, 1).wait_recv()
        t1_copy(e, 1, 1).wait_recv()
        for q in range(parts):
            inner = slice(q * piece, (q + 1) * piece)
            for i in range(2):
                dxacc[e, strip(col, q), halves[i]] += t1r[e, i, 1, inner].astype(F32)

    def arrive(e, q):
        for i in range(2):
            t2_copy(e, i, q).wait_recv()
            dxacc[e, strip(col, q), halves[i]] += t2r[e, i, q].astype(F32)

    def dg_send(i, fs, tp):
        return remote(dgs.at[i], dgr, sent.at[4], dg_recv.at[0], fs, tp)

    def down_parts():
        @pl.when(home)
        def _():
            give.wait_recv()
        take_extra.wait_recv()
        for e in range(2):
            for c in range(chunks):
                remote(hid.at[e, 1 - me, :, lanes_of(c)], hid.at[e, 1 - me, :, lanes_of(c)],
                       sent.at[3], hid_recv.at[e, c], z, sib).wait_recv()
        for i in range(2):
            k = rows_of(2 * core + i)
            value = (jnp.dot(cot_ref[k, :], hid[0, 0], preferred_element_type=F32)
                     + jnp.dot(pcot[k, :], hid[0, 1], preferred_element_type=F32)
                     + jnp.dot(ecot[0, k, :], hid[1, 0], preferred_element_type=F32)
                     + jnp.dot(ecot[1, k, :], hid[1, 1], preferred_element_type=F32))

            @pl.when(jnp.logical_and(home, zodd == i))
            def _():
                dgacc[...] = value

            @pl.when(jnp.logical_and(home, zodd != i))
            def _():
                dgs[0] = value.astype(BF16)

            @pl.when(away)
            def _():
                dgs[i] = value.astype(BF16)

    def down_sends():
        @pl.when(home)
        def _():
            dg_send(0, zs, b).start()

        @pl.when(away)
        def _():
            for i in range(2):
                dg_send(i, 2 * (1 - side) + i, sib).start()
    @pl.when(near)
    def _():
        for c in range(chunks - 1):
            gather(c)
            work(0, c)
        spread_rest(1)
        give_extra.start()
        tok[1] = etok[...].T
        cot[1] = ecot[me].T
        for c in range(chunks - 1):
            work(1, c)
        gather(chunks - 1)
        work_last(1, chunks - 1, True)
        work_last(0, chunks - 1, False)
        down_parts()
        second_step(1)
        for i, step in ((0, 0), (1, 0), (0, 1), (1, 1)):
            t1_copy(0, i, step).start()
        collect(1)
        for q in range(parts):
            arrive(1, q)
            t3s[1, q] = dxacc[1, strip(col, q), :].astype(BF16)

            @pl.when(home)
            def _():
                t3_copy(1, 0, q, zs).start()

            @pl.when(away)
            def _():
                t3_copy(1, 1, q, zf).start()
        down_sends()
        second_step(0)
        collect(0)
        for q in range(parts):
            arrive(0, q)

            @pl.when(away)
            def _():
                t3s[0, q] = dxacc[0, strip(col, q), :].astype(BF16)
                t3_copy(0, 0, q, zn).start()

            @pl.when(jnp.logical_and(home, core == 0))
            def _():
                own_copy(q).start()

    def y_copy(i, k, q, tp):
        ref = ybuf.at[strip(k, q)]
        return remote(ref, ref, sent.at[8], y_recv.at[i, q], z, tp)

    def y_sib(i, k, q):
        ref = ybuf.at[strip(k, q)]
        return remote(ref, ref, sent.at[9], y_recv.at[i, q], z, sib)

    def put(k, q):
        r = strip(k, q)
        return pltpu.make_async_copy(ybuf.at[r], dx_out.at[r], local_sem.at[3])

    dg_put = pltpu.make_async_copy(dgacc, dg_out, local_sem.at[4])

    def result(q, value):
        ybuf[strip(col, q), :] = value.astype(BF16)
    @pl.when(lead)
    def _():
        for q in range(parts):
            t3_copy(0, 0, q, zn).wait_recv()

            @pl.when(end)
            def _():
                t3_copy(1, 1, q, zn).wait_recv()
                result(q, t3r[0, q].astype(F32) + t3r[1, q].astype(F32))

            @pl.when(jnp.logical_and(near, home))
            def _():
                result(q, dxacc[0, strip(col, q), :] + t3r[0, q].astype(F32))

            @pl.when(jnp.logical_and(near, away))
            def _():
                own_copy(q).wait_recv()
                result(q, ownr[q] + t3r[0, q].astype(F32))

            y_copy(2, col, q, bd).start()
            y_copy(0, col, q, bx).start()
            y_copy(1, col, q, by).start()
            y_sib(0, col, q).start()
            put(col, q).start()
        for q in range(parts):
            for i, k, tp in ((0, col_x, bx), (1, col_y, by), (2, col_d, bd)):
                y_copy(i, k, q, tp).wait_recv()
                y_sib(i + 1, k, q).start()
                put(k, q).start()
    @pl.when(jnp.logical_or(end, away))
    def _():
        dg_send(0, zs, b).wait_recv()
        dgacc[...] = dgr[...].astype(F32)

    dg_put.start()
    @pl.when(core == 0)
    def _():
        for q in range(parts):
            for i, k in enumerate((col, col_x, col_y, col_d)):
                y_sib(i, k, q).wait_recv()
                put(k, q).start()
    @pl.when(lead)
    def _():
        drain(ybuf.at[pl.ds(0, 3 * shard)], sent.at[8])
        drain(ybuf, sent.at[9])

    @pl.when(jnp.logical_or(end, away))
    def _():
        drain(weights.at[pl.ds(0, shard)], sent.at[0])

    @pl.when(end)
    def _():
        drain(tally.at[pl.ds(0, 2 * shard)], sent.at[2])

    @pl.when(near)
    def _():
        drain(hid.at[:, 0], sent.at[3])
        drain(t1s, sent.at[5])
        drain(t2s, sent.at[6])

        @pl.when(home)
        def _():
            drain(weights, sent.at[1])
            drain(tally.at[pl.ds(0, 9 * shard)], sent.at[2])
            drain(dgs.at[0], sent.at[4])
            drain(t3s.at[0], sent.at[7])

            @pl.when(core == 0)
            def _():
                drain(ownr, sent.at[10])

        @pl.when(away)
        def _():
            drain(tally, sent.at[2])
            drain(dgs, sent.at[4])
            drain(t3s, sent.at[7])

    drain(ybuf, local_sem.at[3])
    dg_put.wait()


def per_device_kernel(n, tokens, cotangent, gate_weight, up_weight, down_weight):
    rows, depth = tokens.shape
    shard, ff = gate_weight.shape
    chunks = ff // LANES
    parts = next(p for p in (3, 2, 1) if shard % (p * SUB) == 0)
    piece = shard // parts
    vmem, dma = pltpu.VMEM, pltpu.SemaphoreType.DMA
    dx, dg = pl.pallas_call(
        functools.partial(kernel, n),
        out_shape=(vmem((depth, rows), BF16), vmem((shard, ff), F32)),
        in_specs=[pl.BlockSpec(memory_space=pltpu.HBM)] * 5,
        out_specs=[pl.BlockSpec(memory_space=pl.ANY)] * 2,
        scratch_shapes=[
            vmem((depth, rows), BF16), vmem((depth, rows), BF16),
            vmem((shard, ff), BF16), vmem((shard, ff), BF16), vmem((shard, ff), BF16),
            vmem((depth, 3 * ff), BF16),
            vmem((2, rows, depth), BF16), vmem((2, rows, depth), BF16),
            vmem((depth, rows), BF16), vmem((depth, rows), BF16),
            vmem((depth, rows), BF16), vmem((2, depth, rows), BF16),
            vmem((2, depth, rows), F32),
            vmem((2, 2, rows, ff), BF16),
            vmem((shard, ff), F32), vmem((2, shard, ff), BF16), vmem((shard, ff), BF16),
            vmem((2, 2, 2, shard, rows // 2), BF16), vmem((2, 2, 2, shard, rows // 2), BF16),
            vmem((2, 2, parts, piece, rows // 2), BF16), vmem((2, 2, parts, piece, rows // 2), BF16),
            vmem((2, parts, piece, rows), BF16), vmem((2, parts, piece, rows), BF16),
            vmem((parts, piece, rows), F32),
            vmem((depth, rows), BF16),
            vmem((17 * shard, rows), BF16),
            dma((11,)), dma((chunks, 3, 3)), dma((18,)), dma((2, chunks)), dma((1,)),
            dma((2, 2, 2)), dma((2, 2, parts)), dma((2, parts)), dma((parts,)),
            dma((4, parts)), dma((5,)),
        ],
        compiler_params=pltpu.CompilerParams(
            collective_id=0, has_side_effects=True, vmem_limit_bytes=40 * 2**20),
    )(*(pltpu.with_memory_space_constraint(a, pltpu.HBM) for a in (
        tokens.T, cotangent.T, gate_weight, up_weight, down_weight.T)))
    return dx.T, dg.T


def solution(mesh):
    n, tp = mesh.shape["fs"], mesh.shape["tp"]

    def per_device(tokens, cotangent, gate_weight, up_weight, down_weight):
        rows, depth = tokens.shape
        shard, ff = gate_weight.shape
        args = (tokens, cotangent, gate_weight, up_weight, down_weight)
        fits = (tp == 8 and n == 4 and rows % (2 * LANES) == 0 and rows <= 256
                and depth == n * shard and shard % SUB == 0 and ff % LANES == 0
                and LANES < ff <= 512 and depth <= 2048)
        return per_device_kernel(n, *args) if fits else per_device_plain(*args)

    placed = (P("fs", None), P("fs", None), P("fs", "tp"), P("fs", "tp"), P("tp", "fs"))
    return jax.shard_map(
        per_device,
        mesh=mesh,
        in_specs=placed,
        out_specs=(P("fs", None), P("tp", "fs")),
        check_vma=False,
    )
```

time: 61.3 us -> 61.5 us (level)
  the two profiles are of different devices: /device:TPU:0 before, /device:TPU:9 now
where the time goes in v4:
time: 61.5 us; the launch traced here: 61.3 us
  Pallas kernels  59.1 us (96%)
  local copies, waits for them, and re-layouts  1.64 us (3%)
  between operations  0.64 us (1%)
    pallas_call x1, Pallas kernels, per_device_kernel(): pl.pallas_call(functools.partial(kernel, n), out_shape=(vmem((depth, rows...  59.1 us
    unnamed x2, local copies, waits for them, and re-layouts  1.64 us

profile of v4, /device:TPU:9, one launch (start us, length us, event | category | flops | bytes accessed | tf_op | source)
XLA Modules:
  0.0 61.3 jit_solution(17278701721781217583)
XLA Ops:
  0.6 59.1 %shard_map.68 = (bf16[1344,256]{1,0:T(8,128)(2,1)S(1)}, f32[336,384]{1,0:T(8,128)S(1)}) custom-call(bf16[1344,256]{1,0:T(8,128)(2,1)} %bitcast.7, bf16[1344,256]{1,0:T(8,128)(2,1)} %bitcast.8, bf16[336,384]{1,0:T(8,128)(2,1)} %gate_hbm.1, bf16[336,384]{1,0:T(8,128)(2,1)} %up_hbm.1, bf16[336,384]{1,0:T(8,128)(2,1)} %bitcast.9), custom_call_target="tpu_custom_call" | custom-call | tf_op jit(solution)/shard_map/pallas_call | solution.py:505
  59.7 0.8 %copy.9 = bf16[256,1344]{0,1:T(8,128)(2,1)} copy(bf16[256,1344]{0,1:T(8,128)(2,1)S(1)} %bitcast.5) | data formatting | bytes 1376256
  60.5 0.8 %copy.10 = f32[384,336]{0,1:T(8,128)} copy(f32[384,336]{0,1:T(8,128)S(1)} %bitcast.6) | data formatting | bytes 1032192

commit v5 on v4

--- a/solution.py
+++ b/solution.py
@@ -55,9 +55,9 @@
 
 def kernel(n, tok_hbm, cot_hbm, gate_hbm, up_hbm, down_hbm, dx_out, dg_out,
            tok_ref, cot_ref, gate_ref, up_ref, down_ref, weights, tok, cot,
-           ptok, pcot, etok, ecot, dxacc, hid, dgacc, dgs, dgr,
+           ptok, pcot, etok, ecot, dxacc, hid, dgacc, dgp, dgs, dgr, dgf,
            t1s, t1r, t2s, t2r, t3s, t3r, ownr, ybuf, tally,
-           sent, w_recv, tk_recv, hid_recv, dg_recv, t1_recv, t2_recv,
+           sent, w_recv, tk_recv, hid_recv, dg_recv, dgf_recv, t1_recv, t2_recv,
            t3_recv, own_recv, y_recv, local_sem):
     z = lax.axis_index("fs")
     b = lax.axis_index("tp")
@@ -130,8 +130,8 @@
     def own(c, kind):
         return (gate_ref, up_ref, down_ref)[kind].at[:, lanes_of(c)]
 
-    def w_copy(c, k, kind, i, fs):
-        return remote(own(c, kind), slot(c, k, kind), sent.at[0], w_recv.at[c, i, kind], fs, b)
+    def w_copy(src, c, k, kind, i, fs):
+        return remote(src, slot(c, k, kind), sent.at[0], w_recv.at[c, i, kind], fs, b)
 
     def sib_copy(src, c, k, kind):
         return remote(src, slot(c, k, kind), sent.at[1], w_recv.at[c, 0, 0], z, sib)
@@ -147,7 +147,7 @@
         return etok if e else ptok
 
     def cot_buf(e):
-        return ecot.at[me] if e else pcot
+        return ecot if e else pcot
 
     def spread(i, e, q, tp):
         buf = cot_buf(e) if i in (1, 4, 5, 7) else tok_buf(e)
@@ -176,28 +176,47 @@
 
     far_rows = rows_of(2 * (1 - core), 2)
     give = tk_copy(16, pcot.at[far_rows], pcot.at[far_rows], z, sib)
-    give_extra = tk_copy(17, ecot.at[me, far_rows], ecot.at[me, far_rows], z, sib)
-    take_extra = tk_copy(17, ecot.at[1 - me, far_rows], ecot.at[1 - me, far_rows], z, sib)
-    @pl.when(jnp.logical_and(end, home))
-    def _():
-        tk_copy(8, tok_ref.at[mine_q], etok.at[mine_q], zn, b).start()
-        tk_copy(8, tok_ref.at[mine_q], etok.at[mine_q], zs, b).start()
+    give_extra = tk_copy(17, ecot.at[far_rows], ecot.at[far_rows], z, sib)
+    half_me = pl.ds(pl.multiple_of(me * half_rows, LANES), half_rows)
+    @pl.when(end)
+    def _():
+        @pl.when(home)
+        def _():
+            tk_copy(8, tok_ref.at[mine_q], etok.at[mine_q], zn, sib).start()
+
+        @pl.when(away)
+        def _():
+            tk_copy(9, cot_ref.at[mine_q], ecot.at[mine_q], zn, b).start()
+
+    @pl.when(near)
+    def _():
+        @pl.when(home)
+        def _():
+            tk_copy(0, tok_ref.at[mine_q], ptok.at[mine_q], zn, b).start()
+
+        @pl.when(away)
+        def _():
+            tk_copy(1, cot_ref.at[mine_q], pcot.at[mine_q], zn, sib).start()
+
+    @pl.when(home)
+    def _():
         for c, kind in every:
-            w_copy(c, z, kind, 0, zs).start()
-
-    @pl.when(jnp.logical_and(end, away))
-    def _():
-        tk_copy(9, cot_ref.at[mine_q], ecot.at[1, mine_q], zn, sib).start()
-        tk_copy(9, cot_ref.at[mine_q], ecot.at[0, mine_q], zs, sib).start()
-        for c, kind in every:
-            w_copy(c, z, kind, 2, zn).start()
-
-    @pl.when(jnp.logical_and(near, home))
-    def _():
-        tk_copy(0, tok_ref.at[mine_q], ptok.at[mine_q], zn, b).start()
-        for c, kind in every:
+            w_copy(own(c, kind), c, z, kind, 0, zs).start()
             sib_copy(own(c, kind), c, z, kind).start()
             pltpu.make_async_copy(own(c, kind), slot(c, z, kind), local_sem.at[2]).start()
+
+    @pl.when(away)
+    def _():
+        for c, kind in every:
+            w_copy(own(c, kind), c, z, kind, jnp.where(near, 1, 2), zn).start()
+
+    @pl.when(end)
+    def _():
+        tok[0, :half_rows] = tok_ref[:, half_me].T
+        cot[0, :half_rows] = cot_ref[:, half_me].T
+
+    @pl.when(jnp.logical_and(near, home))
+    def _():
         tok[0] = tok_ref[...].T
         cot[0] = cot_ref[...].T
         spread_first(1)
@@ -205,13 +224,8 @@
 
     @pl.when(jnp.logical_and(near, away))
     def _():
-        tk_copy(1, cot_ref.at[mine_q], pcot.at[mine_q], zn, sib).start()
-        for c, kind in every:
-            w_copy(c, z, kind, 1, zn).start()
         spread_first(0)
-        spread_first(1)
         spread_second(0)
-        spread_second(1)
         spread_rest(0)
         give.start()
         tok[0] = ptok[...].T
@@ -222,8 +236,13 @@
         def _():
             for kind in range(3):
                 for i, k in enumerate(others):
-                    w_copy(c, k, kind, i, zs).wait_recv()
-                    sib_copy(slot(c, k, kind), c, k, kind).start()
+                    there = slot(c, k, kind)
+                    w_copy(there, c, k, kind, i, zs).wait_recv()
+                    if i:
+                        @pl.when(near)
+                        def _():
+                            w_copy(there, c, k, kind, i, zs).start()
+                    sib_copy(there, c, k, kind).start()
             if c == 0:
                 drain(weights.at[rows_of(z)], local_sem.at[2])
 
@@ -231,32 +250,45 @@
         def _():
             drain(weights.at[:, lanes_of(3 * c, 3)], w_recv.at[c, 0, 0])
 
-    def hid_copy(e, c):
-        ref = hid.at[e, me, :, lanes_of(c)]
+    def hid_copy(e, c, ref):
         return remote(ref, ref, sent.at[3], hid_recv.at[e, c], z, sib)
 
-    def activate(e, c):
-        pre = jnp.dot(tok[e], weights[:, 3 * c * LANES:(3 * c + 2) * LANES],
+    def hid_ref(e, c):
+        return hid.at[2 if e else me, :, lanes_of(c)]
+
+    def hid_half(c):
+        return hid.at[0, pl.ds(pl.multiple_of(me * half_rows, SUB), half_rows), lanes_of(c)]
+
+    def activate(x, y, c, out, e):
+        pre = jnp.dot(x, weights[:, 3 * c * LANES:(3 * c + 2) * LANES],
                       preferred_element_type=F32)
-        hg = jnp.dot(cot[e], weights[:, (3 * c + 2) * LANES:(3 * c + 3) * LANES],
+        hg = jnp.dot(y, weights[:, (3 * c + 2) * LANES:(3 * c + 3) * LANES],
                      preferred_element_type=F32)
         gate_pre, up_pre = pre[:, :LANES], pre[:, LANES:]
         sig = jax.nn.sigmoid(gate_pre)
         act = gate_pre * sig
-        hid[e, me, :, lanes_of(c)] = (act * up_pre).astype(BF16)
-        hid_copy(e, c).start()
+        out[...] = (act * up_pre).astype(BF16)
+        hid_copy(e, c, out).start()
         return jnp.concatenate(
             [(hg * up_pre * sig * (1.0 + gate_pre * (1.0 - sig))).astype(BF16),
              (hg * act).astype(BF16)], axis=1)
 
     def work(e, c):
-        dgu = activate(e, c)
+        dgu = activate(tok[e], cot[e], c, hid_ref(e, c), e)
         value = contract_cols(weights[:, 3 * c * LANES:(3 * c + 2) * LANES], dgu)
         if c == 0:
             dxacc[e] = value
         else:
             dxacc[e] += value
 
+    def work_half(c):
+        dgu = activate(tok[0, :half_rows], cot[0, :half_rows], c, hid_half(c), 0)
+        value = contract_cols(weights[:, 3 * c * LANES:(3 * c + 2) * LANES], dgu)
+        if c == 0:
+            dxacc[0, :, half_me] = value
+        else:
+            dxacc[0, :, half_me] += value
+
     halves = (slice(0, half_rows), slice(half_rows, rows))
 
     def t1_copy(e, i, step):
@@ -267,8 +299,8 @@
         return remote(t2s.at[e, i, q], t2r.at[e, i, q], sent.at[6], t2_recv.at[e, i, q],
                       z, by if i == 0 else bx)
 
-    def t3_copy(e, i, q, fs):
-        return remote(t3s.at[e, q], t3r.at[i, q], sent.at[7], t3_recv.at[i, q], fs, last)
+    def t3_copy(q, fs):
+        return remote(t3s.at[q], t3r.at[q], sent.at[7], t3_recv.at[q], fs, last)
 
     def strip(k, q):
         return pl.ds(pl.multiple_of(k * shard + q * piece, SUB), piece)
@@ -276,19 +308,64 @@
     def own_copy(q):
         return remote(dxacc.at[0, strip(col, q)], ownr.at[q], sent.at[10], own_recv.at[q], z, sib)
 
-    def work_last(e, c, at_once):
-        dgu = activate(e, c)
+    def work_last(e, c):
+        dgu = activate(tok[e], cot[e], c, hid_ref(e, c), e)
         for k, sends in ((col_d, ((0, 0), (1, 0))), (col_x, ((0, 1),)), (col_y, ((1, 1),)), (col, ())):
             r = rows_of(k)
-            value = contract_cols(weights[r, 3 * c * LANES:(3 * c + 2) * LANES], dgu)
-            if c:
-                value = value + dxacc[e, r, :]
+            value = contract_cols(weights[r, 3 * c * LANES:(3 * c + 2) * LANES], dgu) + dxacc[e, r, :]
             if k is not col_d:
                 dxacc[e, r, :] = value
             for i, step in sends:
                 t1s[e, i, step] = value[:, halves[i]].astype(BF16)
-                if at_once:
-                    t1_copy(e, i, step).start()
+                t1_copy(e, i, step).start()
+
+    first_tp = jnp.where(home, bx, by)
+    second_tp = jnp.where(home, by, bx)
+    first_col = jnp.where(home, col_x, col_y)
+    second_col = jnp.where(home, col_y, col_x)
+
+    def t1_half(step):
+        return remote(t1s.at[0, me, step], t1r.at[0, me, step], sent.at[5], t1_recv.at[0, me, step],
+                      z, first_tp)
+
+    def t2_half(q):
+        return remote(t2s.at[0, me, q], t2r.at[0, me, q], sent.at[6], t2_recv.at[0, me, q],
+                      z, second_tp)
+
+    def own_half(q):
+        return remote(dxacc.at[0, strip(col, q), half_me], ownr.at[q, :, half_me],
+                      sent.at[10], own_recv.at[q], z, sib)
+
+    def last_half(c):
+        dgu = activate(tok[0, :half_rows], cot[0, :half_rows], c, hid_half(c), 0)
+        for k, step in ((col_d, 0), (first_col, 1), (second_col, 2), (col, 2)):
+            r = rows_of(k)
+            value = (contract_cols(weights[r, 3 * c * LANES:(3 * c + 2) * LANES], dgu)
+                     + dxacc[0, r, half_me])
+            if step:
+                dxacc[0, r, half_me] = value
+            if step < 2:
+                t1s[0, me, step] = value.astype(BF16)
+                t1_half(step).start()
+
+    def reduce_half():
+        t1_half(0).wait_recv()
+        for q in range(parts):
+            inner = slice(q * piece, (q + 1) * piece)
+            t2s[0, me, q] = (dxacc[0, strip(second_col, q), half_me]
+                             + t1r[0, me, 0, inner].astype(F32)).astype(BF16)
+            t2_half(q).start()
+        t1_half(1).wait_recv()
+        for q in range(parts):
+            inner = slice(q * piece, (q + 1) * piece)
+            dxacc[0, strip(col, q), half_me] += t1r[0, me, 1, inner].astype(F32)
+        for q in range(parts):
+            t2_half(q).wait_recv()
+            dxacc[0, strip(col, q), half_me] += t2r[0, me, q].astype(F32)
+
+            @pl.when(core == 0)
+            def _():
+                own_half(q).start()
 
     def second_step(e):
         t1_copy(e, 0, 0).wait_recv()
@@ -313,91 +390,160 @@
             t2_copy(e, i, q).wait_recv()
             dxacc[e, strip(col, q), halves[i]] += t2r[e, i, q].astype(F32)
 
-    def dg_send(i, fs, tp):
-        return remote(dgs.at[i], dgr, sent.at[4], dg_recv.at[0], fs, tp)
-
-    def down_parts():
-        @pl.when(home)
-        def _():
-            give.wait_recv()
-        take_extra.wait_recv()
-        for e in range(2):
-            for c in range(chunks):
-                remote(hid.at[e, 1 - me, :, lanes_of(c)], hid.at[e, 1 - me, :, lanes_of(c)],
-                       sent.at[3], hid_recv.at[e, c], z, sib).wait_recv()
+    stages = (slice(0, ff - LANES), slice(ff - LANES, ff))
+
+    def lanes_at(g):
+        return pl.ds(stages[g].start, stages[g].stop - stages[g].start)
+
+    def dg_home(g):
+        lanes = lanes_at(g)
+        return remote(dgs.at[0, :, lanes], dgr.at[0, :, lanes], sent.at[4], dg_recv.at[g], zs, b)
+
+    def dg_away(g):
+        lanes = lanes_at(g)
+        return remote(dgs.at[:, :, lanes], dgr.at[:, :, lanes], sent.at[4], dg_recv.at[g], zs, b)
+
+    def dg_far(g, i):
+        lanes = lanes_at(g)
+        return remote(dgs.at[i, :, lanes], dgf.at[:, lanes], sent.at[4], dgf_recv.at[g],
+                      2 * (1 - side) + i, sib)
+
+    def stage_chunks(g):
+        return range(chunks - 1) if g == 0 else (chunks - 1,)
+
+    def keep_part(g, i, value):
+        lanes = stages[g]
+
+        @pl.when(jnp.logical_and(home, zodd == i))
+        def _():
+            dgacc[:, lanes] = value
+
+        @pl.when(jnp.logical_and(home, zodd != i))
+        def _():
+            dgs[0, :, lanes] = value.astype(BF16)
+
+        @pl.when(jnp.logical_and(away, near))
+        def _():
+            dgp[i, :, lanes] = value
+
+        @pl.when(jnp.logical_and(away, end))
+        def _():
+            dgs[i, :, lanes] = value.astype(BF16)
+
+    def down_near(g):
+        for c in stage_chunks(g):
+            hid_copy(0, c, hid.at[1 - me, :, lanes_of(c)]).wait_recv()
+
+            @pl.when(away)
+            def _():
+                hid_copy(1, c, hid.at[2, :, lanes_of(c)]).wait_recv()
+        lanes = stages[g]
         for i in range(2):
             k = rows_of(2 * core + i)
-            value = (jnp.dot(cot_ref[k, :], hid[0, 0], preferred_element_type=F32)
-                     + jnp.dot(pcot[k, :], hid[0, 1], preferred_element_type=F32)
-                     + jnp.dot(ecot[0, k, :], hid[1, 0], preferred_element_type=F32)
-                     + jnp.dot(ecot[1, k, :], hid[1, 1], preferred_element_type=F32))
-
-            @pl.when(jnp.logical_and(home, zodd == i))
-            def _():
-                dgacc[...] = value
-
-            @pl.when(jnp.logical_and(home, zodd != i))
-            def _():
-                dgs[0] = value.astype(BF16)
-
-            @pl.when(away)
-            def _():
-                dgs[i] = value.astype(BF16)
-
-    def down_sends():
-        @pl.when(home)
-        def _():
-            dg_send(0, zs, b).start()
+            keep_part(g, i, jnp.dot(cot_ref[k, :], hid[0, :, lanes], preferred_element_type=F32)
+                      + jnp.dot(pcot[k, :], hid[1, :, lanes], preferred_element_type=F32)
+                      + jnp.dot(ecot[k, :], hid[2, :, lanes], preferred_element_type=F32))
+
+        @pl.when(home)
+        def _():
+            dg_home(g).start()
+
+    def down_end(g):
+        for c in stage_chunks(g):
+            other = hid.at[0, pl.ds(pl.multiple_of((1 - me) * half_rows, SUB), half_rows), lanes_of(c)]
+            hid_copy(0, c, other).wait_recv()
+        for i in range(2):
+            k = rows_of(2 * core + i)
+            keep_part(g, i, jnp.dot(cot_ref[k, :], hid[0, :, stages[g]], preferred_element_type=F32))
+
+        @pl.when(home)
+        def _():
+            dg_home(g).start()
 
         @pl.when(away)
         def _():
-            for i in range(2):
-                dg_send(i, 2 * (1 - side) + i, sib).start()
+            dg_away(g).start()
+
+    def down_mid(g):
+        lanes = stages[g]
+        dg_away(g).wait_recv()
+        for i in range(2):
+            dgs[i, :, lanes] = (dgp[i, :, lanes] + dgr[i, :, lanes].astype(F32)).astype(BF16)
+            dg_far(g, i).start()
     @pl.when(near)
     def _():
         for c in range(chunks - 1):
             gather(c)
             work(0, c)
-        spread_rest(1)
-        give_extra.start()
-        tok[1] = etok[...].T
-        cot[1] = ecot[me].T
-        for c in range(chunks - 1):
-            work(1, c)
+
+        @pl.when(home)
+        def _():
+            spread_rest(1)
+            give_extra.start()
+            tok[1] = etok[...].T
+            cot[1] = ecot[...].T
+            for c in range(chunks - 1):
+                work(1, c)
         gather(chunks - 1)
-        work_last(1, chunks - 1, True)
-        work_last(0, chunks - 1, False)
-        down_parts()
-        second_step(1)
-        for i, step in ((0, 0), (1, 0), (0, 1), (1, 1)):
-            t1_copy(0, i, step).start()
-        collect(1)
-        for q in range(parts):
-            arrive(1, q)
-            t3s[1, q] = dxacc[1, strip(col, q), :].astype(BF16)
-
-            @pl.when(home)
-            def _():
-                t3_copy(1, 0, q, zs).start()
+
+        @pl.when(home)
+        def _():
+            work_last(1, chunks - 1)
+        work_last(0, chunks - 1)
+
+        @pl.when(home)
+        def _():
+            give.wait_recv()
+
+        @pl.when(away)
+        def _():
+            give_extra.wait_recv()
+
+        down_near(0)
+
+        @pl.when(away)
+        def _():
+            down_mid(0)
+
+        down_near(1)
+
+        @pl.when(home)
+        def _():
+            second_step(1)
+            collect(1)
+            for q in range(parts):
+                arrive(1, q)
+                t3s[q] = dxacc[1, strip(col, q), :].astype(BF16)
+                t3_copy(q, zf).start()
+        second_step(0)
+        collect(0)
+        for q in range(parts):
+            arrive(0, q)
 
             @pl.when(away)
             def _():
-                t3_copy(1, 1, q, zf).start()
-        down_sends()
-        second_step(0)
-        collect(0)
-        for q in range(parts):
-            arrive(0, q)
-
-            @pl.when(away)
-            def _():
-                t3s[0, q] = dxacc[0, strip(col, q), :].astype(BF16)
-                t3_copy(0, 0, q, zn).start()
+                t3s[q] = dxacc[0, strip(col, q), :].astype(BF16)
+                t3_copy(q, zn).start()
 
             @pl.when(jnp.logical_and(home, core == 0))
             def _():
                 own_copy(q).start()
 
+        @pl.when(away)
+        def _():
+            down_mid(1)
+
+    @pl.when(end)
+    def _():
+        for c in range(chunks - 1):
+            gather(c)
+            work_half(c)
+        down_end(0)
+        gather(chunks - 1)
+        last_half(chunks - 1)
+        down_end(1)
+        reduce_half()
+
     def y_copy(i, k, q, tp):
         ref = ybuf.at[strip(k, q)]
         return remote(ref, ref, sent.at[8], y_recv.at[i, q], z, tp)
@@ -417,22 +563,24 @@
     @pl.when(lead)
     def _():
         for q in range(parts):
-            t3_copy(0, 0, q, zn).wait_recv()
+            t3_copy(q, zn).wait_recv()
 
             @pl.when(end)
             def _():
-                t3_copy(1, 1, q, zn).wait_recv()
-                result(q, t3r[0, q].astype(F32) + t3r[1, q].astype(F32))
+                own_half(q).wait_recv()
+                there = pl.ds(pl.multiple_of((1 - me) * half_rows, LANES), half_rows)
+                r = strip(col, q)
+                ybuf[r, half_me] = (dxacc[0, r, half_me] + t3r[q, :, half_me].astype(F32)).astype(BF16)
+                ybuf[r, there] = (ownr[q, :, there] + t3r[q, :, there].astype(F32)).astype(BF16)
 
             @pl.when(jnp.logical_and(near, home))
             def _():
-                result(q, dxacc[0, strip(col, q), :] + t3r[0, q].astype(F32))
+                result(q, dxacc[0, strip(col, q), :] + t3r[q].astype(F32))
 
             @pl.when(jnp.logical_and(near, away))
             def _():
                 own_copy(q).wait_recv()
-                result(q, ownr[q] + t3r[0, q].astype(F32))
-
+                result(q, ownr[q] + t3r[q].astype(F32))
             y_copy(2, col, q, bd).start()
             y_copy(0, col, q, bx).start()
             y_copy(1, col, q, by).start()
@@ -443,10 +591,17 @@
                 y_copy(i, k, q, tp).wait_recv()
                 y_sib(i + 1, k, q).start()
                 put(k, q).start()
-    @pl.when(jnp.logical_or(end, away))
-    def _():
-        dg_send(0, zs, b).wait_recv()
-        dgacc[...] = dgr[...].astype(F32)
+    @pl.when(home)
+    def _():
+        for g in range(2):
+            dg_home(g).wait_recv()
+        dgacc[...] += dgr[0].astype(F32)
+
+    @pl.when(away)
+    def _():
+        for g in range(2):
+            dg_far(g, 0).wait_recv()
+        dgacc[...] = dgf[...].astype(F32)
 
     dg_put.start()
     @pl.when(core == 0)
@@ -460,26 +615,42 @@
         drain(ybuf.at[pl.ds(0, 3 * shard)], sent.at[8])
         drain(ybuf, sent.at[9])
 
-    @pl.when(jnp.logical_or(end, away))
+    @pl.when(home)
+    def _():
+        drain(weights, sent.at[1])
+        drain(dgs.at[0], sent.at[4])
+
+    @pl.when(away)
     def _():
         drain(weights.at[pl.ds(0, shard)], sent.at[0])
+        drain(dgs, sent.at[4])
 
     @pl.when(end)
     def _():
-        drain(tally.at[pl.ds(0, 2 * shard)], sent.at[2])
+        drain(tally.at[pl.ds(0, shard)], sent.at[2])
+        drain(hid.at[0, pl.ds(0, half_rows)], sent.at[3])
+        drain(t1s.at[0, 0], sent.at[5])
+        drain(t2s.at[0, 0], sent.at[6])
+
+        @pl.when(home)
+        def _():
+            drain(weights.at[pl.ds(0, shard)], sent.at[0])
+
+        @pl.when(core == 0)
+        def _():
+            drain(ownr.at[:, :, pl.ds(0, half_rows)], sent.at[10])
 
     @pl.when(near)
     def _():
-        drain(hid.at[:, 0], sent.at[3])
-        drain(t1s, sent.at[5])
-        drain(t2s, sent.at[6])
-
-        @pl.when(home)
-        def _():
-            drain(weights, sent.at[1])
-            drain(tally.at[pl.ds(0, 9 * shard)], sent.at[2])
-            drain(dgs.at[0], sent.at[4])
-            drain(t3s.at[0], sent.at[7])
+        drain(tally, sent.at[2])
+        drain(t3s, sent.at[7])
+
+        @pl.when(home)
+        def _():
+            drain(weights.at[pl.ds(0, 3 * shard)], sent.at[0])
+            drain(hid.at[pl.ds(0, 2)], sent.at[3])
+            drain(t1s, sent.at[5])
+            drain(t2s, sent.at[6])
 
             @pl.when(core == 0)
             def _():
@@ -487,9 +658,9 @@
 
         @pl.when(away)
         def _():
-            drain(tally, sent.at[2])
-            drain(dgs, sent.at[4])
-            drain(t3s, sent.at[7])
+            drain(hid.at[0], sent.at[3])
+            drain(t1s.at[0], sent.at[5])
+            drain(t2s.at[0], sent.at[6])
 
     drain(ybuf, local_sem.at[3])
     dg_put.wait()
@@ -513,18 +684,19 @@
             vmem((depth, 3 * ff), BF16),
             vmem((2, rows, depth), BF16), vmem((2, rows, depth), BF16),
             vmem((depth, rows), BF16), vmem((depth, rows), BF16),
-            vmem((depth, rows), BF16), vmem((2, depth, rows), BF16),
+            vmem((depth, rows), BF16), vmem((depth, rows), BF16),
             vmem((2, depth, rows), F32),
-            vmem((2, 2, rows, ff), BF16),
-            vmem((shard, ff), F32), vmem((2, shard, ff), BF16), vmem((shard, ff), BF16),
+            vmem((3, rows, ff), BF16),
+            vmem((shard, ff), F32), vmem((2, shard, ff), F32), vmem((2, shard, ff), BF16),
+            vmem((2, shard, ff), BF16), vmem((shard, ff), BF16),
             vmem((2, 2, 2, shard, rows // 2), BF16), vmem((2, 2, 2, shard, rows // 2), BF16),
             vmem((2, 2, parts, piece, rows // 2), BF16), vmem((2, 2, parts, piece, rows // 2), BF16),
-            vmem((2, parts, piece, rows), BF16), vmem((2, parts, piece, rows), BF16),
+            vmem((parts, piece, rows), BF16), vmem((parts, piece, rows), BF16),
             vmem((parts, piece, rows), F32),
             vmem((depth, rows), BF16),
-            vmem((17 * shard, rows), BF16),
-            dma((11,)), dma((chunks, 3, 3)), dma((18,)), dma((2, chunks)), dma((1,)),
-            dma((2, 2, 2)), dma((2, 2, parts)), dma((2, parts)), dma((parts,)),
+            vmem((9 * shard, rows), BF16),
+            dma((11,)), dma((chunks, 3, 3)), dma((18,)), dma((2, chunks)), dma((2,)), dma((2,)),
+            dma((2, 2, 2)), dma((2, 2, parts)), dma((parts,)), dma((parts,)),
             dma((4, parts)), dma((5,)),
         ],
         compiler_params=pltpu.CompilerParams(

time: 61.5 us -> 58.1 us (0.945)
  the two profiles are of different devices: /device:TPU:9 before, /device:TPU:0 now
where the time goes in v5:
time: 58.1 us; the launch traced here: 57.1 us
  Pallas kernels  54.9 us (94%)
  local copies, waits for them, and re-layouts  1.64 us (3%)
  between operations  0.64 us (1%)
    pallas_call x1, Pallas kernels, per_device_kernel(): pl.pallas_call(functools.partial(kernel, n), out_shape=(vmem((depth, rows...  54.9 us
    unnamed x2, local copies, waits for them, and re-layouts  1.64 us

profile of v5, /device:TPU:0, one launch (start us, length us, event | category | flops | bytes accessed | tf_op | source)
XLA Modules:
  0.0 57.1 jit_solution(14462614779294588409)
XLA Ops:
  0.6 54.9 %shard_map.68 = (bf16[1344,256]{1,0:T(8,128)(2,1)S(1)}, f32[336,384]{1,0:T(8,128)S(1)}) custom-call(bf16[1344,256]{1,0:T(8,128)(2,1)} %bitcast.7, bf16[1344,256]{1,0:T(8,128)(2,1)} %bitcast.8, bf16[336,384]{1,0:T(8,128)(2,1)} %gate_hbm.1, bf16[336,384]{1,0:T(8,128)(2,1)} %up_hbm.1, bf16[336,384]{1,0:T(8,128)(2,1)} %bitcast.9), custom_call_target="tpu_custom_call" | custom-call | tf_op jit(solution)/shard_map/pallas_call | solution.py:676
  55.5 0.8 %copy.9 = bf16[256,1344]{0,1:T(8,128)(2,1)} copy(bf16[256,1344]{0,1:T(8,128)(2,1)S(1)} %bitcast.5) | data formatting | bytes 1376256
  56.4 0.8 %copy.10 = f32[384,336]{0,1:T(8,128)} copy(f32[384,336]{0,1:T(8,128)S(1)} %bitcast.6) | data formatting | bytes 1032192

commit v6 on v5

--- a/solution.py
+++ b/solution.py
@@ -326,15 +326,16 @@
 
     def t1_half(step):
         return remote(t1s.at[0, me, step], t1r.at[0, me, step], sent.at[5], t1_recv.at[0, me, step],
-                      z, first_tp)
-
-    def t2_half(q):
-        return remote(t2s.at[0, me, q], t2r.at[0, me, q], sent.at[6], t2_recv.at[0, me, q],
-                      z, second_tp)
-
-    def own_half(q):
-        return remote(dxacc.at[0, strip(col, q), half_me], ownr.at[q, :, half_me],
-                      sent.at[10], own_recv.at[q], z, sib)
+                      z, first_tp + 1 - core)
+
+    def own_half(i, k):
+        ref = dxacc.at[0, rows_of(k), half_me]
+        return remote(ref, ref, sent.at[10], own_recv.at[i], z, sib)
+
+    def take_half(i, k):
+        there = pl.ds(pl.multiple_of((1 - me) * half_rows, LANES), half_rows)
+        ref = dxacc.at[0, rows_of(k), there]
+        return remote(ref, ref, sent.at[10], own_recv.at[i], z, sib)
 
     def last_half(c):
         dgu = activate(tok[0, :half_rows], cot[0, :half_rows], c, hid_half(c), 0)
@@ -349,23 +350,19 @@
                 t1_half(step).start()
 
     def reduce_half():
-        t1_half(0).wait_recv()
-        for q in range(parts):
-            inner = slice(q * piece, (q + 1) * piece)
-            t2s[0, me, q] = (dxacc[0, strip(second_col, q), half_me]
-                             + t1r[0, me, 0, inner].astype(F32)).astype(BF16)
-            t2_half(q).start()
-        t1_half(1).wait_recv()
-        for q in range(parts):
-            inner = slice(q * piece, (q + 1) * piece)
-            dxacc[0, strip(col, q), half_me] += t1r[0, me, 1, inner].astype(F32)
-        for q in range(parts):
-            t2_half(q).wait_recv()
-            dxacc[0, strip(col, q), half_me] += t2r[0, me, q].astype(F32)
-
-            @pl.when(core == 0)
-            def _():
-                own_half(q).start()
+        @pl.when(core == 0)
+        def _():
+            own_half(0, second_col).start()
+            own_half(1, col).start()
+
+        @pl.when(lead)
+        def _():
+            take_half(0, first_col).wait_recv()
+            second_step(0)
+            take_half(1, col).wait_recv()
+            collect(0)
+            for q in range(parts):
+                arrive(0, q)
 
     def second_step(e):
         t1_copy(e, 0, 0).wait_recv()
@@ -444,10 +441,6 @@
                       + jnp.dot(pcot[k, :], hid[1, :, lanes], preferred_element_type=F32)
                       + jnp.dot(ecot[k, :], hid[2, :, lanes], preferred_element_type=F32))
 
-        @pl.when(home)
-        def _():
-            dg_home(g).start()
-
     def down_end(g):
         for c in stage_chunks(g):
             other = hid.at[0, pl.ds(pl.multiple_of((1 - me) * half_rows, SUB), half_rows), lanes_of(c)]
@@ -475,6 +468,7 @@
         for c in range(chunks - 1):
             gather(c)
             work(0, c)
+        gather(chunks - 1)
 
         @pl.when(home)
         def _():
@@ -484,7 +478,6 @@
             cot[1] = ecot[...].T
             for c in range(chunks - 1):
                 work(1, c)
-        gather(chunks - 1)
 
         @pl.when(home)
         def _():
@@ -499,13 +492,8 @@
         def _():
             give_extra.wait_recv()
 
-        down_near(0)
-
-        @pl.when(away)
-        def _():
-            down_mid(0)
-
-        down_near(1)
+        for g in range(2):
+            down_near(g)
 
         @pl.when(home)
         def _():
@@ -515,6 +503,8 @@
                 arrive(1, q)
                 t3s[q] = dxacc[1, strip(col, q), :].astype(BF16)
                 t3_copy(q, zf).start()
+            for g in range(2):
+                dg_home(g).start()
         second_step(0)
         collect(0)
         for q in range(parts):
@@ -531,7 +521,11 @@
 
         @pl.when(away)
         def _():
-            down_mid(1)
+            down_mid(0)
+
+            @pl.when(core == 0)
+            def _():
+                down_mid(1)
 
     @pl.when(end)
     def _():
@@ -565,15 +559,7 @@
         for q in range(parts):
             t3_copy(q, zn).wait_recv()
 
-            @pl.when(end)
-            def _():
-                own_half(q).wait_recv()
-                there = pl.ds(pl.multiple_of((1 - me) * half_rows, LANES), half_rows)
-                r = strip(col, q)
-                ybuf[r, half_me] = (dxacc[0, r, half_me] + t3r[q, :, half_me].astype(F32)).astype(BF16)
-                ybuf[r, there] = (ownr[q, :, there] + t3r[q, :, there].astype(F32)).astype(BF16)
-
-            @pl.when(jnp.logical_and(near, home))
+            @pl.when(jnp.logical_or(end, home))
             def _():
                 result(q, dxacc[0, strip(col, q), :] + t3r[q].astype(F32))
 
@@ -586,6 +572,10 @@
             y_copy(1, col, q, by).start()
             y_sib(0, col, q).start()
             put(col, q).start()
+
+        @pl.when(jnp.logical_and(near, away))
+        def _():
+            down_mid(1)
         for q in range(parts):
             for i, k, tp in ((0, col_x, bx), (1, col_y, by), (2, col_d, bd)):
                 y_copy(i, k, q, tp).wait_recv()
@@ -630,7 +620,10 @@
         drain(tally.at[pl.ds(0, shard)], sent.at[2])
         drain(hid.at[0, pl.ds(0, half_rows)], sent.at[3])
         drain(t1s.at[0, 0], sent.at[5])
-        drain(t2s.at[0, 0], sent.at[6])
+
+        @pl.when(lead)
+        def _():
+            drain(t2s.at[0], sent.at[6])
 
         @pl.when(home)
         def _():
@@ -638,7 +631,7 @@
 
         @pl.when(core == 0)
         def _():
-            drain(ownr.at[:, :, pl.ds(0, half_rows)], sent.at[10])
+            drain(dxacc.at[0, pl.ds(0, 2 * shard), pl.ds(0, half_rows)], sent.at[10])
 
     @pl.when(near)
     def _():

time: 58.1 us -> 55.8 us (0.960); the launches traced: 57.1 us -> 55.6 us
  Pallas kernels: 54.9 us -> 53.4 us
    pallas_call x1, Pallas kernels: 54.9 us -> 53.4 us  [per_device_kernel(): pl.pallas_call(functools.partial(kernel, n), out_shape=(vmem((depth, rows...]
where the time goes in v6:
time: 55.8 us; the launch traced here: 55.6 us
  Pallas kernels  53.4 us (96%)
  local copies, waits for them, and re-layouts  1.64 us (3%)
  between operations  0.64 us (1%)
    pallas_call x1, Pallas kernels, per_device_kernel(): pl.pallas_call(functools.partial(kernel, n), out_shape=(vmem((depth, rows...  53.4 us
    unnamed x2, local copies, waits for them, and re-layouts  1.64 us

profile of v6, /device:TPU:0, one launch (start us, length us, event | category | flops | bytes accessed | tf_op | source)
XLA Modules:
  0.0 55.6 jit_solution(18227171356786650268)
XLA Ops:
  0.6 53.4 %shard_map.68 = (bf16[1344,256]{1,0:T(8,128)(2,1)S(1)}, f32[336,384]{1,0:T(8,128)S(1)}) custom-call(bf16[1344,256]{1,0:T(8,128)(2,1)} %bitcast.7, bf16[1344,256]{1,0:T(8,128)(2,1)} %bitcast.8, bf16[336,384]{1,0:T(8,128)(2,1)} %gate_hbm.1, bf16[336,384]{1,0:T(8,128)(2,1)} %up_hbm.1, bf16[336,384]{1,0:T(8,128)(2,1)} %bitcast.9), custom_call_target="tpu_custom_call" | custom-call | tf_op jit(solution)/shard_map/pallas_call | solution.py:669
  54.0 0.8 %copy.9 = bf16[256,1344]{0,1:T(8,128)(2,1)} copy(bf16[256,1344]{0,1:T(8,128)(2,1)S(1)} %bitcast.5) | data formatting | bytes 1376256
  54.8 0.8 %copy.10 = f32[384,336]{0,1:T(8,128)} copy(f32[384,336]{0,1:T(8,128)S(1)} %bitcast.6) | data formatting | bytes 1032192

commit v7 on v6

--- a/solution.py
+++ b/solution.py
@@ -55,10 +55,10 @@
 
 def kernel(n, tok_hbm, cot_hbm, gate_hbm, up_hbm, down_hbm, dx_out, dg_out,
            tok_ref, cot_ref, gate_ref, up_ref, down_ref, weights, tok, cot,
-           ptok, pcot, etok, ecot, dxacc, hid, dgacc, dgp, dgs, dgr, dgf,
-           t1s, t1r, t2s, t2r, t3s, t3r, ownr, ybuf, tally,
-           sent, w_recv, tk_recv, hid_recv, dg_recv, dgf_recv, t1_recv, t2_recv,
-           t3_recv, own_recv, y_recv, local_sem):
+           ptok, pcot, etok, ecot, dxacc, hid, dgacc, dgp, dgs, dgr, dgf, dge,
+           t1s, t1r, t2s, t2r, t3s, t3r, es, er, ownr, ybuf, tally,
+           sent, w_recv, tk_recv, hid_recv, dg_recv, dgf_recv, dge_recv, t1_recv, t2_recv,
+           t3_recv, e_recv, own_recv, y_recv, local_sem):
     z = lax.axis_index("fs")
     b = lax.axis_index("tp")
     depth, rows = tok_ref.shape
@@ -231,24 +231,33 @@
         tok[0] = ptok[...].T
         cot[0] = pcot[...].T
 
+    def relay(c, kind):
+        for i, k in enumerate(others):
+            there = slot(c, k, kind)
+            w_copy(there, c, k, kind, i, zs).wait_recv()
+            if i:
+                @pl.when(near)
+                def _():
+                    w_copy(there, c, k, kind, i, zs).start()
+            sib_copy(there, c, k, kind).start()
+
+    def relay_all(c):
+        for kind in range(3):
+            relay(c, kind)
+        if c == 0:
+            drain(weights.at[rows_of(z)], local_sem.at[2])
+
+    def gather_sib(c):
+        drain(weights.at[:, lanes_of(3 * c, 3)], w_recv.at[c, 0, 0])
+
     def gather(c):
         @pl.when(home)
         def _():
-            for kind in range(3):
-                for i, k in enumerate(others):
-                    there = slot(c, k, kind)
-                    w_copy(there, c, k, kind, i, zs).wait_recv()
-                    if i:
-                        @pl.when(near)
-                        def _():
-                            w_copy(there, c, k, kind, i, zs).start()
-                    sib_copy(there, c, k, kind).start()
-            if c == 0:
-                drain(weights.at[rows_of(z)], local_sem.at[2])
-
-        @pl.when(away)
-        def _():
-            drain(weights.at[:, lanes_of(3 * c, 3)], w_recv.at[c, 0, 0])
+            relay_all(c)
+
+        @pl.when(away)
+        def _():
+            gather_sib(c)
 
     def hid_copy(e, c, ref):
         return remote(ref, ref, sent.at[3], hid_recv.at[e, c], z, sib)
@@ -273,13 +282,21 @@
             [(hg * up_pre * sig * (1.0 + gate_pre * (1.0 - sig))).astype(BF16),
              (hg * act).astype(BF16)], axis=1)
 
-    def work(e, c):
-        dgu = activate(tok[e], cot[e], c, hid_ref(e, c), e)
+    def begin(e, c):
+        return activate(tok[e], cot[e], c, hid_ref(e, c), e)
+
+    def finish(e, c, dgu):
         value = contract_cols(weights[:, 3 * c * LANES:(3 * c + 2) * LANES], dgu)
         if c == 0:
             dxacc[e] = value
         else:
             dxacc[e] += value
+
+    def take_tokens():
+        spread_rest(1)
+        give_extra.start()
+        tok[1] = etok[...].T
+        cot[1] = ecot[...].T
 
     def work_half(c):
         dgu = activate(tok[0, :half_rows], cot[0, :half_rows], c, hid_half(c), 0)
@@ -319,50 +336,42 @@
                 t1s[e, i, step] = value[:, halves[i]].astype(BF16)
                 t1_copy(e, i, step).start()
 
-    first_tp = jnp.where(home, bx, by)
-    second_tp = jnp.where(home, by, bx)
-    first_col = jnp.where(home, col_x, col_y)
-    second_col = jnp.where(home, col_y, col_x)
-
-    def t1_half(step):
-        return remote(t1s.at[0, me, step], t1r.at[0, me, step], sent.at[5], t1_recv.at[0, me, step],
-                      z, first_tp + 1 - core)
-
-    def own_half(i, k):
-        ref = dxacc.at[0, rows_of(k), half_me]
-        return remote(ref, ref, sent.at[10], own_recv.at[i], z, sib)
-
-    def take_half(i, k):
-        there = pl.ds(pl.multiple_of((1 - me) * half_rows, LANES), half_rows)
-        ref = dxacc.at[0, rows_of(k), there]
-        return remote(ref, ref, sent.at[10], own_recv.at[i], z, sib)
+    there = pl.ds(pl.multiple_of((1 - me) * half_rows, LANES), half_rows)
+
+    def e_copy(i, q, tp):
+        return remote(es.at[i, q], er.at[q, me, i], sent.at[5], e_recv.at[q], z, tp + 1 - core)
+
+    def own_half():
+        ref = dxacc.at[0, rows_of(col), half_me]
+        return remote(ref, ref, sent.at[10], own_recv.at[0], z, sib)
+
+    def take_half():
+        ref = dxacc.at[0, rows_of(col), there]
+        return remote(ref, ref, sent.at[10], own_recv.at[0], z, sib)
 
     def last_half(c):
         dgu = activate(tok[0, :half_rows], cot[0, :half_rows], c, hid_half(c), 0)
-        for k, step in ((col_d, 0), (first_col, 1), (second_col, 2), (col, 2)):
-            r = rows_of(k)
-            value = (contract_cols(weights[r, 3 * c * LANES:(3 * c + 2) * LANES], dgu)
-                     + dxacc[0, r, half_me])
-            if step:
-                dxacc[0, r, half_me] = value
-            if step < 2:
-                t1s[0, me, step] = value.astype(BF16)
-                t1_half(step).start()
-
-    def reduce_half():
+        columns = pl.ds(3 * c * LANES, 2 * LANES)
+        for q in range(parts):
+            for i, (k, tp) in enumerate(((col_d, bd), (col_x, bx), (col_y, by))):
+                r = strip(k, q)
+                es[i, q] = (contract_cols(weights[r, columns], dgu) + dxacc[0, r, half_me]).astype(BF16)
+                e_copy(i, q, tp).start()
+        r = rows_of(col)
+        dxacc[0, r, half_me] += contract_cols(weights[r, columns], dgu)
+
         @pl.when(core == 0)
         def _():
-            own_half(0, second_col).start()
-            own_half(1, col).start()
-
-        @pl.when(lead)
-        def _():
-            take_half(0, first_col).wait_recv()
-            second_step(0)
-            take_half(1, col).wait_recv()
-            collect(0)
-            for q in range(parts):
-                arrive(0, q)
+            own_half().start()
+
+    def end_result(q):
+        drain(er.at[q], e_recv.at[q])
+        r = strip(col, q)
+        for i in range(2):
+            total = dxacc[0, r, halves[i]] + t3r[q, :, halves[i]].astype(F32)
+            for k in range(3):
+                total = total + er[q, i, k].astype(F32)
+            ybuf[r, halves[i]] = total.astype(BF16)
 
     def second_step(e):
         t1_copy(e, 0, 0).wait_recv()
@@ -387,29 +396,28 @@
             t2_copy(e, i, q).wait_recv()
             dxacc[e, strip(col, q), halves[i]] += t2r[e, i, q].astype(F32)
 
-    stages = (slice(0, ff - LANES), slice(ff - LANES, ff))
-
-    def lanes_at(g):
-        return pl.ds(stages[g].start, stages[g].stop - stages[g].start)
+    def span(c):
+        return slice(c * LANES, (c + 1) * LANES)
 
     def dg_home(g):
-        lanes = lanes_at(g)
+        lanes = lanes_of(g)
         return remote(dgs.at[0, :, lanes], dgr.at[0, :, lanes], sent.at[4], dg_recv.at[g], zs, b)
 
     def dg_away(g):
-        lanes = lanes_at(g)
+        lanes = lanes_of(g)
         return remote(dgs.at[:, :, lanes], dgr.at[:, :, lanes], sent.at[4], dg_recv.at[g], zs, b)
 
     def dg_far(g, i):
-        lanes = lanes_at(g)
+        lanes = lanes_of(g)
         return remote(dgs.at[i, :, lanes], dgf.at[:, lanes], sent.at[4], dgf_recv.at[g],
                       2 * (1 - side) + i, sib)
 
-    def stage_chunks(g):
-        return range(chunks - 1) if g == 0 else (chunks - 1,)
+    def dg_direct(i):
+        return remote(dgs.at[i, :, lanes_of(chunks - 1)], dge, sent.at[4], dge_recv.at[0],
+                      2 * (1 - side) + i, sib)
 
     def keep_part(g, i, value):
-        lanes = stages[g]
+        lanes = span(g)
 
         @pl.when(jnp.logical_and(home, zodd == i))
         def _():
@@ -419,22 +427,35 @@
         def _():
             dgs[0, :, lanes] = value.astype(BF16)
 
-        @pl.when(jnp.logical_and(away, near))
-        def _():
-            dgp[i, :, lanes] = value
-
-        @pl.when(jnp.logical_and(away, end))
-        def _():
-            dgs[i, :, lanes] = value.astype(BF16)
+        if g == chunks - 1:
+            @pl.when(away)
+            def _():
+                dgs[i, :, lanes] = value.astype(BF16)
+
+                @pl.when(near)
+                def _():
+                    dg_far(g, i).start()
+
+                @pl.when(end)
+                def _():
+                    dg_direct(i).start()
+        else:
+            @pl.when(jnp.logical_and(away, near))
+            def _():
+                dgp[i, :, lanes] = value
+
+            @pl.when(jnp.logical_and(away, end))
+            def _():
+                dgs[i, :, lanes] = value.astype(BF16)
 
     def down_near(g):
-        for c in stage_chunks(g):
-            hid_copy(0, c, hid.at[1 - me, :, lanes_of(c)]).wait_recv()
-
-            @pl.when(away)
-            def _():
-                hid_copy(1, c, hid.at[2, :, lanes_of(c)]).wait_recv()
-        lanes = stages[g]
+        hid_copy(0, g, hid.at[1 - me, :, lanes_of(g)]).wait_recv()
+
+        @pl.when(away)
+        def _():
+            hid_copy(1, g, hid.at[2, :, lanes_of(g)]).wait_recv()
+
+        lanes = span(g)
         for i in range(2):
             k = rows_of(2 * core + i)
             keep_part(g, i, jnp.dot(cot_ref[k, :], hid[0, :, lanes], preferred_element_type=F32)
@@ -442,42 +463,49 @@
                       + jnp.dot(ecot[k, :], hid[2, :, lanes], preferred_element_type=F32))
 
     def down_end(g):
-        for c in stage_chunks(g):
-            other = hid.at[0, pl.ds(pl.multiple_of((1 - me) * half_rows, SUB), half_rows), lanes_of(c)]
-            hid_copy(0, c, other).wait_recv()
+        other = hid.at[0, pl.ds(pl.multiple_of((1 - me) * half_rows, SUB), half_rows), lanes_of(g)]
+        hid_copy(0, g, other).wait_recv()
         for i in range(2):
             k = rows_of(2 * core + i)
-            keep_part(g, i, jnp.dot(cot_ref[k, :], hid[0, :, stages[g]], preferred_element_type=F32))
+            keep_part(g, i, jnp.dot(cot_ref[k, :], hid[0, :, span(g)], preferred_element_type=F32))
 
         @pl.when(home)
         def _():
             dg_home(g).start()
 
-        @pl.when(away)
-        def _():
-            dg_away(g).start()
+        if g < chunks - 1:
+            @pl.when(away)
+            def _():
+                dg_away(g).start()
 
     def down_mid(g):
-        lanes = stages[g]
+        lanes = span(g)
         dg_away(g).wait_recv()
         for i in range(2):
             dgs[i, :, lanes] = (dgp[i, :, lanes] + dgr[i, :, lanes].astype(F32)).astype(BF16)
             dg_far(g, i).start()
     @pl.when(near)
     def _():
-        for c in range(chunks - 1):
-            gather(c)
-            work(0, c)
-        gather(chunks - 1)
-
-        @pl.when(home)
-        def _():
-            spread_rest(1)
-            give_extra.start()
-            tok[1] = etok[...].T
-            cot[1] = ecot[...].T
+
+        @pl.when(home)
+        def _():
+            relay_all(0)
             for c in range(chunks - 1):
-                work(1, c)
+                dgu = begin(0, c)
+                relay(c + 1, 0)
+                finish(0, c, dgu)
+                if c == 0:
+                    take_tokens()
+                relay(c + 1, 1)
+                finish(1, c, begin(1, c))
+                relay(c + 1, 2)
+
+        @pl.when(away)
+        def _():
+            for c in range(chunks - 1):
+                gather_sib(c)
+                finish(0, c, begin(0, c))
+            gather_sib(chunks - 1)
 
         @pl.when(home)
         def _():
@@ -486,26 +514,36 @@
 
         @pl.when(home)
         def _():
-            give.wait_recv()
-
-        @pl.when(away)
-        def _():
-            give_extra.wait_recv()
-
-        for g in range(2):
-            down_near(g)
-
-        @pl.when(home)
-        def _():
             second_step(1)
             collect(1)
+
+        @pl.when(home)
+        def _():
+            give.wait_recv()
+
+        @pl.when(away)
+        def _():
+            give_extra.wait_recv()
+
+        for c in range(chunks):
+            down_near(c)
+
+            @pl.when(home)
+            def _():
+                dg_home(c).start()
+
+            if c == 0 and chunks > 2:
+                @pl.when(away)
+                def _():
+                    down_mid(0)
+        second_step(0)
+
+        @pl.when(home)
+        def _():
             for q in range(parts):
                 arrive(1, q)
                 t3s[q] = dxacc[1, strip(col, q), :].astype(BF16)
                 t3_copy(q, zf).start()
-            for g in range(2):
-                dg_home(g).start()
-        second_step(0)
         collect(0)
         for q in range(parts):
             arrive(0, q)
@@ -521,22 +559,22 @@
 
         @pl.when(away)
         def _():
-            down_mid(0)
-
-            @pl.when(core == 0)
-            def _():
-                down_mid(1)
+            for c in range(0 if chunks == 2 else 1, chunks - 1):
+                down_mid(c)
 
     @pl.when(end)
     def _():
         for c in range(chunks - 1):
             gather(c)
             work_half(c)
-        down_end(0)
+            down_end(c)
         gather(chunks - 1)
         last_half(chunks - 1)
-        down_end(1)
-        reduce_half()
+        down_end(chunks - 1)
+
+        @pl.when(lead)
+        def _():
+            take_half().wait_recv()
 
     def y_copy(i, k, q, tp):
         ref = ybuf.at[strip(k, q)]
@@ -554,12 +592,33 @@
 
     def result(q, value):
         ybuf[strip(col, q), :] = value.astype(BF16)
+
+    def down_final():
+        @pl.when(home)
+        def _():
+            for g in range(chunks):
+                dg_home(g).wait_recv()
+            dgacc[...] += dgr[0].astype(F32)
+
+        @pl.when(away)
+        def _():
+            for g in range(chunks):
+                dg_far(g, 0).wait_recv()
+            dg_direct(0).wait_recv()
+            dgacc[...] = dgf[...].astype(F32)
+            dgacc[:, span(chunks - 1)] += dge[...].astype(F32)
+
+        dg_put.start()
     @pl.when(lead)
     def _():
         for q in range(parts):
             t3_copy(q, zn).wait_recv()
 
-            @pl.when(jnp.logical_or(end, home))
+            @pl.when(end)
+            def _():
+                end_result(q)
+
+            @pl.when(jnp.logical_and(near, home))
             def _():
                 result(q, dxacc[0, strip(col, q), :] + t3r[q].astype(F32))
 
@@ -572,30 +631,15 @@
             y_copy(1, col, q, by).start()
             y_sib(0, col, q).start()
             put(col, q).start()
-
-        @pl.when(jnp.logical_and(near, away))
-        def _():
-            down_mid(1)
+        down_final()
         for q in range(parts):
             for i, k, tp in ((0, col_x, bx), (1, col_y, by), (2, col_d, bd)):
                 y_copy(i, k, q, tp).wait_recv()
                 y_sib(i + 1, k, q).start()
                 put(k, q).start()
-    @pl.when(home)
-    def _():
-        for g in range(2):
-            dg_home(g).wait_recv()
-        dgacc[...] += dgr[0].astype(F32)
-
-    @pl.when(away)
-    def _():
-        for g in range(2):
-            dg_far(g, 0).wait_recv()
-        dgacc[...] = dgf[...].astype(F32)
-
-    dg_put.start()
     @pl.when(core == 0)
     def _():
+        down_final()
         for q in range(parts):
             for i, k in enumerate((col, col_x, col_y, col_d)):
                 y_sib(i, k, q).wait_recv()
@@ -619,11 +663,7 @@
     def _():
         drain(tally.at[pl.ds(0, shard)], sent.at[2])
         drain(hid.at[0, pl.ds(0, half_rows)], sent.at[3])
-        drain(t1s.at[0, 0], sent.at[5])
-
-        @pl.when(lead)
-        def _():
-            drain(t2s.at[0], sent.at[6])
+        drain(es, sent.at[5])
 
         @pl.when(home)
         def _():
@@ -631,7 +671,7 @@
 
         @pl.when(core == 0)
         def _():
-            drain(dxacc.at[0, pl.ds(0, 2 * shard), pl.ds(0, half_rows)], sent.at[10])
+            drain(dxacc.at[0, pl.ds(0, shard), pl.ds(0, half_rows)], sent.at[10])
 
     @pl.when(near)
     def _():
@@ -681,15 +721,16 @@
             vmem((2, depth, rows), F32),
             vmem((3, rows, ff), BF16),
             vmem((shard, ff), F32), vmem((2, shard, ff), F32), vmem((2, shard, ff), BF16),
-            vmem((2, shard, ff), BF16), vmem((shard, ff), BF16),
+            vmem((2, shard, ff), BF16), vmem((shard, ff), BF16), vmem((shard, LANES), BF16),
             vmem((2, 2, 2, shard, rows // 2), BF16), vmem((2, 2, 2, shard, rows // 2), BF16),
             vmem((2, 2, parts, piece, rows // 2), BF16), vmem((2, 2, parts, piece, rows // 2), BF16),
             vmem((parts, piece, rows), BF16), vmem((parts, piece, rows), BF16),
+            vmem((3, parts, piece, rows // 2), BF16), vmem((parts, 2, 3, piece, rows // 2), BF16),
             vmem((parts, piece, rows), F32),
             vmem((depth, rows), BF16),
             vmem((9 * shard, rows), BF16),
-            dma((11,)), dma((chunks, 3, 3)), dma((18,)), dma((2, chunks)), dma((2,)), dma((2,)),
-            dma((2, 2, 2)), dma((2, 2, parts)), dma((parts,)), dma((parts,)),
+            dma((11,)), dma((chunks, 3, 3)), dma((18,)), dma((2, chunks)), dma((chunks,)), dma((chunks,)), dma((1,)),
+            dma((2, 2, 2)), dma((2, 2, parts)), dma((parts,)), dma((parts,)), dma((parts,)),
             dma((4, parts)), dma((5,)),
         ],
         compiler_params=pltpu.CompilerParams(

time: 55.8 us -> 54.9 us (0.984)
  Pallas kernels: 53.4 us -> 52.5 us
    pallas_call x1, Pallas kernels: 53.4 us -> 52.5 us  [per_device_kernel(): pl.pallas_call(functools.partial(kernel, n), out_shape=(vmem((depth, rows...]
where the time goes in v7:
time: 54.9 us; the launch traced here: 54.8 us
  Pallas kernels  52.5 us (96%)
  local copies, waits for them, and re-layouts  1.64 us (3%)
  between operations  0.64 us (1%)
    pallas_call x1, Pallas kernels, per_device_kernel(): pl.pallas_call(functools.partial(kernel, n), out_shape=(vmem((depth, rows...  52.5 us
    unnamed x2, local copies, waits for them, and re-layouts  1.64 us

profile of v7, /device:TPU:0, one launch (start us, length us, event | category | flops | bytes accessed | tf_op | source)
XLA Modules:
  0.0 54.8 jit_solution(16873069107351180417)
XLA Ops:
  0.6 52.5 %shard_map.68 = (bf16[1344,256]{1,0:T(8,128)(2,1)S(1)}, f32[336,384]{1,0:T(8,128)S(1)}) custom-call(bf16[1344,256]{1,0:T(8,128)(2,1)} %bitcast.7, bf16[1344,256]{1,0:T(8,128)(2,1)} %bitcast.8, bf16[336,384]{1,0:T(8,128)(2,1)} %gate_hbm.1, bf16[336,384]{1,0:T(8,128)(2,1)} %up_hbm.1, bf16[336,384]{1,0:T(8,128)(2,1)} %bitcast.9), custom_call_target="tpu_custom_call" | custom-call | tf_op jit(solution)/shard_map/pallas_call | solution.py:709
  53.1 0.8 %copy.9 = bf16[256,1344]{0,1:T(8,128)(2,1)} copy(bf16[256,1344]{0,1:T(8,128)(2,1)S(1)} %bitcast.5) | data formatting | bytes 1376256
  54.0 0.8 %copy.10 = f32[384,336]{0,1:T(8,128)} copy(f32[384,336]{0,1:T(8,128)S(1)} %bitcast.6) | data formatting | bytes 1032192

commit v8 on v7

--- a/solution.py
+++ b/solution.py
@@ -53,10 +53,10 @@
     return (input_grad, down_grad)
 
 
-def kernel(n, tok_hbm, cot_hbm, gate_hbm, up_hbm, down_hbm, dx_out, dg_out,
+def kernel(n, tok_hbm, cot_hbm, gate_hbm, up_hbm, down_hbm, ybuf, dgacc,
            tok_ref, cot_ref, gate_ref, up_ref, down_ref, weights, tok, cot,
-           ptok, pcot, etok, ecot, dxacc, hid, dgacc, dgp, dgs, dgr, dgf, dge,
-           t1s, t1r, t2s, t2r, t3s, t3r, es, er, ownr, ybuf, tally,
+           ptok, pcot, etok, ecot, dxacc, hid, dgp, dgs, dgr, dgf, dge,
+           t1s, t1r, t2s, t2r, t3s, t3r, es, er, ownr, tally,
            sent, w_recv, tk_recv, hid_recv, dg_recv, dgf_recv, dge_recv, t1_recv, t2_recv,
            t3_recv, e_recv, own_recv, y_recv, local_sem):
     z = lax.axis_index("fs")
@@ -152,7 +152,7 @@
     def spread(i, e, q, tp):
         buf = cot_buf(e) if i in (1, 4, 5, 7) else tok_buf(e)
         ref = buf.at[rows_of(q)]
-        return tk_copy(8 * e + i, ref, ref, z, tp)
+        return tk_copy(8 * e + (3 if i in (4, 6, 7) else i), ref, ref, z, tp)
 
     def spread_first(e):
         spread(0, e, col, bx).wait_recv()
@@ -169,10 +169,7 @@
         spread(7, e, col_y, bx).start()
 
     def spread_rest(e):
-        spread(3, e, col_y, by).wait_recv()
-        spread(6, e, col_d, by).wait_recv()
-        spread(4, e, col_x, bx).wait_recv()
-        spread(7, e, col_d, bx).wait_recv()
+        drain(tally.at[pl.ds(0, 4 * shard)], tk_recv.at[8 * e + 3])
 
     far_rows = rows_of(2 * (1 - core), 2)
     give = tk_copy(16, pcot.at[far_rows], pcot.at[far_rows], z, sib)
@@ -309,11 +306,11 @@
     halves = (slice(0, half_rows), slice(half_rows, rows))
 
     def t1_copy(e, i, step):
-        return remote(t1s.at[e, i, step], t1r.at[e, i, step], sent.at[5], t1_recv.at[e, i, step],
+        return remote(t1s.at[e, i, step], t1r.at[e, i, step], sent.at[5], t1_recv.at[e, step],
                       z, bx if i == 0 else by)
 
     def t2_copy(e, i, q):
-        return remote(t2s.at[e, i, q], t2r.at[e, i, q], sent.at[6], t2_recv.at[e, i, q],
+        return remote(t2s.at[e, i, q], t2r.at[e, i, q], sent.at[6], t2_recv.at[e, q],
                       z, by if i == 0 else bx)
 
     def t3_copy(q, fs):
@@ -374,8 +371,7 @@
             ybuf[r, halves[i]] = total.astype(BF16)
 
     def second_step(e):
-        t1_copy(e, 0, 0).wait_recv()
-        t1_copy(e, 1, 0).wait_recv()
+        drain(t1r.at[e, :, 0], t1_recv.at[e, 0])
         for q in range(parts):
             inner = slice(q * piece, (q + 1) * piece)
             for i, k in ((0, col_y), (1, col_x)):
@@ -384,16 +380,15 @@
                 t2_copy(e, i, q).start()
 
     def collect(e):
-        t1_copy(e, 0, 1).wait_recv()
-        t1_copy(e, 1, 1).wait_recv()
+        drain(t1r.at[e, :, 1], t1_recv.at[e, 1])
         for q in range(parts):
             inner = slice(q * piece, (q + 1) * piece)
             for i in range(2):
                 dxacc[e, strip(col, q), halves[i]] += t1r[e, i, 1, inner].astype(F32)
 
     def arrive(e, q):
+        drain(t2r.at[e, :, q], t2_recv.at[e, q])
         for i in range(2):
-            t2_copy(e, i, q).wait_recv()
             dxacc[e, strip(col, q), halves[i]] += t2r[e, i, q].astype(F32)
 
     def span(c):
@@ -578,17 +573,11 @@
 
     def y_copy(i, k, q, tp):
         ref = ybuf.at[strip(k, q)]
-        return remote(ref, ref, sent.at[8], y_recv.at[i, q], z, tp)
+        return remote(ref, ref, sent.at[8], y_recv.at[q], z, tp)
 
     def y_sib(i, k, q):
         ref = ybuf.at[strip(k, q)]
-        return remote(ref, ref, sent.at[9], y_recv.at[i, q], z, sib)
-
-    def put(k, q):
-        r = strip(k, q)
-        return pltpu.make_async_copy(ybuf.at[r], dx_out.at[r], local_sem.at[3])
-
-    dg_put = pltpu.make_async_copy(dgacc, dg_out, local_sem.at[4])
+        return remote(ref, ref, sent.at[9], y_recv.at[q], z, sib)
 
     def result(q, value):
         ybuf[strip(col, q), :] = value.astype(BF16)
@@ -607,8 +596,6 @@
             dg_direct(0).wait_recv()
             dgacc[...] = dgf[...].astype(F32)
             dgacc[:, span(chunks - 1)] += dge[...].astype(F32)
-
-        dg_put.start()
     @pl.when(lead)
     def _():
         for q in range(parts):
@@ -630,20 +617,16 @@
             y_copy(0, col, q, bx).start()
             y_copy(1, col, q, by).start()
             y_sib(0, col, q).start()
-            put(col, q).start()
         down_final()
         for q in range(parts):
-            for i, k, tp in ((0, col_x, bx), (1, col_y, by), (2, col_d, bd)):
-                y_copy(i, k, q, tp).wait_recv()
+            drain(tally.at[pl.ds(0, 3 * piece)], y_recv.at[q])
+            for i, k in enumerate((col_x, col_y, col_d)):
                 y_sib(i + 1, k, q).start()
-                put(k, q).start()
     @pl.when(core == 0)
     def _():
         down_final()
         for q in range(parts):
-            for i, k in enumerate((col, col_x, col_y, col_d)):
-                y_sib(i, k, q).wait_recv()
-                put(k, q).start()
+            drain(tally.at[pl.ds(0, 4 * piece)], y_recv.at[q])
     @pl.when(lead)
     def _():
         drain(ybuf.at[pl.ds(0, 3 * shard)], sent.at[8])
@@ -695,8 +678,14 @@
             drain(t1s.at[0], sent.at[5])
             drain(t2s.at[0], sent.at[6])
 
-    drain(ybuf, local_sem.at[3])
-    dg_put.wait()
+
+def store_kernel(dx_in, dg_in, dx_out, dg_out, sem):
+    copies = [pltpu.make_async_copy(src, dst, sem.at[i])
+              for i, (src, dst) in enumerate(((dx_in, dx_out), (dg_in, dg_out)))]
+    for copy in copies:
+        copy.start()
+    for copy in copies:
+        copy.wait()
 
 
 def per_device_kernel(n, tokens, cotangent, gate_weight, up_weight, down_weight):
@@ -710,7 +699,7 @@
         functools.partial(kernel, n),
         out_shape=(vmem((depth, rows), BF16), vmem((shard, ff), F32)),
         in_specs=[pl.BlockSpec(memory_space=pltpu.HBM)] * 5,
-        out_specs=[pl.BlockSpec(memory_space=pl.ANY)] * 2,
+        out_specs=[pl.BlockSpec(memory_space=vmem)] * 2,
         scratch_shapes=[
             vmem((depth, rows), BF16), vmem((depth, rows), BF16),
             vmem((shard, ff), BF16), vmem((shard, ff), BF16), vmem((shard, ff), BF16),
@@ -720,23 +709,30 @@
             vmem((depth, rows), BF16), vmem((depth, rows), BF16),
             vmem((2, depth, rows), F32),
             vmem((3, rows, ff), BF16),
-            vmem((shard, ff), F32), vmem((2, shard, ff), F32), vmem((2, shard, ff), BF16),
+            vmem((2, shard, ff), F32), vmem((2, shard, ff), BF16),
             vmem((2, shard, ff), BF16), vmem((shard, ff), BF16), vmem((shard, LANES), BF16),
             vmem((2, 2, 2, shard, rows // 2), BF16), vmem((2, 2, 2, shard, rows // 2), BF16),
             vmem((2, 2, parts, piece, rows // 2), BF16), vmem((2, 2, parts, piece, rows // 2), BF16),
             vmem((parts, piece, rows), BF16), vmem((parts, piece, rows), BF16),
             vmem((3, parts, piece, rows // 2), BF16), vmem((parts, 2, 3, piece, rows // 2), BF16),
             vmem((parts, piece, rows), F32),
-            vmem((depth, rows), BF16),
             vmem((9 * shard, rows), BF16),
             dma((11,)), dma((chunks, 3, 3)), dma((18,)), dma((2, chunks)), dma((chunks,)), dma((chunks,)), dma((1,)),
-            dma((2, 2, 2)), dma((2, 2, parts)), dma((parts,)), dma((parts,)), dma((parts,)),
-            dma((4, parts)), dma((5,)),
+            dma((2, 2)), dma((2, parts)), dma((parts,)), dma((parts,)), dma((parts,)),
+            dma((parts,)), dma((3,)),
         ],
         compiler_params=pltpu.CompilerParams(
             collective_id=0, has_side_effects=True, vmem_limit_bytes=40 * 2**20),
     )(*(pltpu.with_memory_space_constraint(a, pltpu.HBM) for a in (
         tokens.T, cotangent.T, gate_weight, up_weight, down_weight.T)))
+    dx, dg = pl.pallas_call(
+        store_kernel,
+        out_shape=(pltpu.HBM((depth, rows), BF16), pltpu.HBM((shard, ff), F32)),
+        in_specs=[pl.BlockSpec(memory_space=pl.ANY)] * 2,
+        out_specs=[pl.BlockSpec(memory_space=pl.ANY)] * 2,
+        scratch_shapes=[dma((2,))],
+        compiler_params=pltpu.CompilerParams(vmem_limit_bytes=2**20),
+    )(dx, dg)
     return dx.T, dg.T
 
 

time: 54.9 us -> 54.1 us (0.985)
  local copies, waits for them, and re-layouts: 1.64 us -> 0 us
  Pallas kernels: 52.5 us -> 53.3 us
    unnamed x2 -> x0, local copies, waits for them, and re-layouts: 1.64 us -> none
    pallas_call x0 -> x1, Pallas kernels: none -> 1.03 us  [per_device_kernel(): pl.pallas_call(store_kernel, out_shape=(pltpu.HBM((depth, rows), BF16), p...]
where the time goes in v8:
time: 54.1 us; the launch traced here: 53.9 us
  Pallas kernels  53.3 us (99%)
  between operations  0.64 us (1%)
    pallas_call x1, Pallas kernels, per_device_kernel(): pl.pallas_call(functools.partial(kernel, n), out_shape=(vmem((depth, rows...  52.3 us

profile of v8, /device:TPU:0, one launch (start us, length us, event | category | flops | bytes accessed | tf_op | source)
XLA Modules:
  0.0 53.9 jit_solution(5774836975118619928)
XLA Ops:
  0.6 52.3 %shard_map.68 = (bf16[1344,256]{1,0:T(8,128)(2,1)S(1)}, f32[336,384]{1,0:T(8,128)S(1)}) custom-call(bf16[1344,256]{1,0:T(8,128)(2,1)} %bitcast.5, bf16[1344,256]{1,0:T(8,128)(2,1)} %bitcast.6, bf16[336,384]{1,0:T(8,128)(2,1)} %gate_hbm.1, bf16[336,384]{1,0:T(8,128)(2,1)} %up_hbm.1, bf16[336,384]{1,0:T(8,128)(2,1)} %bitcast.7), custom_call_target="tpu_custom_call" | custom-call | tf_op jit(solution)/shard_map/pallas_call | solution.py:698
  52.9 1.0 %shard_map.69 = (bf16[1344,256]{1,0:T(8,128)(2,1)}, f32[336,384]{1,0:T(8,128)}) custom-call(bf16[1344,256]{1,0:T(8,128)(2,1)S(1)} %get-tuple-element.6.dx_in, f32[336,384]{1,0:T(8,128)S(1)} %get-tuple-element.7.dg_in), custom_call_target="tpu_custom_call" | custom-call | tf_op jit(solution)/shard_map/pallas_call | solution.py:728

commit v9 on v8

--- a/solution.py
+++ b/solution.py
@@ -134,7 +134,7 @@
         return remote(src, slot(c, k, kind), sent.at[0], w_recv.at[c, i, kind], fs, b)
 
     def sib_copy(src, c, k, kind):
-        return remote(src, slot(c, k, kind), sent.at[1], w_recv.at[c, 0, 0], z, sib)
+        return remote(src, slot(c, k, kind), sent.at[1], w_recv.at[c, 0, int(c == chunks - 1 and kind == 2)], z, sib)
 
     every = [(c, kind) for c in range(chunks) for kind in range(3)]
     others = (zs, zn, zf)
@@ -245,7 +245,11 @@
             drain(weights.at[rows_of(z)], local_sem.at[2])
 
     def gather_sib(c):
-        drain(weights.at[:, lanes_of(3 * c, 3)], w_recv.at[c, 0, 0])
+        if c < chunks - 1:
+            drain(weights.at[:, lanes_of(3 * c, 3)], w_recv.at[c, 0, 0])
+        else:
+            drain(weights.at[:, lanes_of(3 * c, 2)], w_recv.at[c, 0, 0])
+            drain(weights.at[:, lanes_of(3 * c + 2)], w_recv.at[c, 0, 1])
 
     def gather(c):
         @pl.when(home)
@@ -265,9 +269,12 @@
     def hid_half(c):
         return hid.at[0, pl.ds(pl.multiple_of(me * half_rows, SUB), half_rows), lanes_of(c)]
 
-    def activate(x, y, c, out, e):
-        pre = jnp.dot(x, weights[:, 3 * c * LANES:(3 * c + 2) * LANES],
-                      preferred_element_type=F32)
+    def gate_up(x, c):
+        return jnp.dot(x, weights[:, 3 * c * LANES:(3 * c + 2) * LANES],
+                       preferred_element_type=F32)
+
+    def activate(x, y, c, out, e, pre=None):
+        pre = gate_up(x, c) if pre is None else pre
         hg = jnp.dot(y, weights[:, (3 * c + 2) * LANES:(3 * c + 3) * LANES],
                      preferred_element_type=F32)
         gate_pre, up_pre = pre[:, :LANES], pre[:, LANES:]
@@ -331,7 +338,13 @@
                 dxacc[e, r, :] = value
             for i, step in sends:
                 t1s[e, i, step] = value[:, halves[i]].astype(BF16)
-                t1_copy(e, i, step).start()
+                if e:
+                    t1_copy(e, i, step).start()
+                else:
+                    @pl.when(away)
+                    def _():
+                        t1_copy(e, i, step).start()
+
 
     there = pl.ds(pl.multiple_of((1 - me) * half_rows, LANES), half_rows)
 
@@ -347,7 +360,25 @@
         return remote(ref, ref, sent.at[10], own_recv.at[0], z, sib)
 
     def last_half(c):
-        dgu = activate(tok[0, :half_rows], cot[0, :half_rows], c, hid_half(c), 0)
+        @pl.when(home)
+        def _():
+            relay(c, 0)
+            relay(c, 1)
+
+        @pl.when(away)
+        def _():
+            drain(weights.at[:, lanes_of(3 * c, 2)], w_recv.at[c, 0, 0])
+
+        pre = gate_up(tok[0, :half_rows], c)
+
+        @pl.when(home)
+        def _():
+            relay(c, 2)
+
+        @pl.when(away)
+        def _():
+            drain(weights.at[:, lanes_of(3 * c + 2)], w_recv.at[c, 0, 1])
+        dgu = activate(tok[0, :half_rows], cot[0, :half_rows], c, hid_half(c), 0, pre)
         columns = pl.ds(3 * c * LANES, 2 * LANES)
         for q in range(parts):
             for i, (k, tp) in enumerate(((col_d, bd), (col_x, bx), (col_y, by))):
@@ -356,7 +387,6 @@
                 e_copy(i, q, tp).start()
         r = rows_of(col)
         dxacc[0, r, half_me] += contract_cols(weights[r, columns], dgu)
-
         @pl.when(core == 0)
         def _():
             own_half().start()
@@ -510,6 +540,9 @@
         @pl.when(home)
         def _():
             second_step(1)
+            for step in range(2):
+                for i in range(2):
+                    t1_copy(0, i, step).start()
             collect(1)
 
         @pl.when(home)
@@ -520,25 +553,27 @@
         def _():
             give_extra.wait_recv()
 
-        for c in range(chunks):
-            down_near(c)
-
-            @pl.when(home)
-            def _():
-                dg_home(c).start()
-
-            if c == 0 and chunks > 2:
-                @pl.when(away)
-                def _():
+        @pl.when(away)
+        def _():
+            for c in range(chunks):
+                down_near(c)
+                if c == 0 and chunks > 2:
                     down_mid(0)
-        second_step(0)
-
-        @pl.when(home)
-        def _():
+            second_step(0)
+
+        @pl.when(home)
+        def _():
+            down_near(0)
+            dg_home(0).start()
             for q in range(parts):
                 arrive(1, q)
                 t3s[q] = dxacc[1, strip(col, q), :].astype(BF16)
                 t3_copy(q, zf).start()
+            second_step(0)
+            for c in range(1, chunks):
+                down_near(c)
+                dg_home(c).start()
+
         collect(0)
         for q in range(parts):
             arrive(0, q)
@@ -563,7 +598,6 @@
             gather(c)
             work_half(c)
             down_end(c)
-        gather(chunks - 1)
         last_half(chunks - 1)
         down_end(chunks - 1)
 

time: 54.1 us -> 53.4 us (0.987)
  Pallas kernels: 53.3 us -> 52.4 us
    pallas_call x1, Pallas kernels: 52.3 us -> 51.4 us  [per_device_kernel(): pl.pallas_call(functools.partial(kernel, n), out_shape=(vmem((depth, rows...]
where the time goes in v9:
time: 53.4 us; the launch traced here: 53.2 us
  Pallas kernels  52.4 us (98%)
  between operations  0.82 us (2%)
    pallas_call x1, Pallas kernels, per_device_kernel(): pl.pallas_call(functools.partial(kernel, n), out_shape=(vmem((depth, rows...  51.4 us

profile of v9, /device:TPU:0, one launch (start us, length us, event | category | flops | bytes accessed | tf_op | source)
XLA Modules:
  0.0 53.2 jit_solution(15431912562832971485)
XLA Ops:
  0.6 51.4 %shard_map.68 = (bf16[1344,256]{1,0:T(8,128)(2,1)S(1)}, f32[336,384]{1,0:T(8,128)S(1)}) custom-call(bf16[1344,256]{1,0:T(8,128)(2,1)} %bitcast.5, bf16[1344,256]{1,0:T(8,128)(2,1)} %bitcast.6, bf16[336,384]{1,0:T(8,128)(2,1)} %gate_hbm.1, bf16[336,384]{1,0:T(8,128)(2,1)} %up_hbm.1, bf16[336,384]{1,0:T(8,128)(2,1)} %bitcast.7), custom_call_target="tpu_custom_call" | custom-call | tf_op jit(solution)/shard_map/pallas_call | solution.py:732
  52.0 1.0 %shard_map.69 = (bf16[1344,256]{1,0:T(8,128)(2,1)}, f32[336,384]{1,0:T(8,128)}) custom-call(bf16[1344,256]{1,0:T(8,128)(2,1)S(1)} %get-tuple-element.6.dx_in, f32[336,384]{1,0:T(8,128)S(1)} %get-tuple-element.7.dg_in), custom_call_target="tpu_custom_call" | custom-call | tf_op jit(solution)/shard_map/pallas_call | solution.py:762

commit v10 on v9

--- a/solution.py
+++ b/solution.py
@@ -714,8 +714,12 @@
 
 
 def store_kernel(dx_in, dg_in, dx_out, dg_out, sem):
-    copies = [pltpu.make_async_copy(src, dst, sem.at[i])
-              for i, (src, dst) in enumerate(((dx_in, dx_out), (dg_in, dg_out)))]
+    copies = []
+    for src, dst in ((dx_in, dx_out), (dg_in, dg_out)):
+        step = src.shape[0] // 3
+        for lo in range(0, 3 * step, step):
+            r = pl.ds(lo, step)
+            copies.append(pltpu.make_async_copy(src.at[r], dst.at[r], sem.at[len(copies)]))
     for copy in copies:
         copy.start()
     for copy in copies:
@@ -764,7 +768,7 @@
         out_shape=(pltpu.HBM((depth, rows), BF16), pltpu.HBM((shard, ff), F32)),
         in_specs=[pl.BlockSpec(memory_space=pl.ANY)] * 2,
         out_specs=[pl.BlockSpec(memory_space=pl.ANY)] * 2,
-        scratch_shapes=[dma((2,))],
+        scratch_shapes=[dma((6,))],
         compiler_params=pltpu.CompilerParams(vmem_limit_bytes=2**20),
     )(dx, dg)
     return dx.T, dg.T
@@ -779,7 +783,7 @@
         args = (tokens, cotangent, gate_weight, up_weight, down_weight)
         fits = (tp == 8 and n == 4 and rows % (2 * LANES) == 0 and rows <= 256
                 and depth == n * shard and shard % SUB == 0 and ff % LANES == 0
-                and LANES < ff <= 512 and depth <= 2048)
+                and shard % 48 == 0 and LANES < ff <= 512 and depth <= 2048)
         return per_device_kernel(n, *args) if fits else per_device_plain(*args)
 
     placed = (P("fs", None), P("fs", None), P("fs", "tp"), P("fs", "tp"), P("tp", "fs"))

time: 53.4 us -> 53.4 us (level)
  no operation moved by 1% of the time
where the time goes in v10:
time: 53.4 us; the launch traced here: 53.2 us
  Pallas kernels  52.4 us (98%)
  between operations  0.82 us (2%)
    pallas_call x1, Pallas kernels, per_device_kernel(): pl.pallas_call(functools.partial(kernel, n), out_shape=(vmem((depth, rows...  51.4 us

profile of v10, /device:TPU:0, one launch (start us, length us, event | category | flops | bytes accessed | tf_op | source)
XLA Modules:
  0.0 53.2 jit_solution(1870141101094648172)
XLA Ops:
  0.6 51.4 %shard_map.68 = (bf16[1344,256]{1,0:T(8,128)(2,1)S(1)}, f32[336,384]{1,0:T(8,128)S(1)}) custom-call(bf16[1344,256]{1,0:T(8,128)(2,1)} %bitcast.5, bf16[1344,256]{1,0:T(8,128)(2,1)} %bitcast.6, bf16[336,384]{1,0:T(8,128)(2,1)} %gate_hbm.1, bf16[336,384]{1,0:T(8,128)(2,1)} %up_hbm.1, bf16[336,384]{1,0:T(8,128)(2,1)} %bitcast.7), custom_call_target="tpu_custom_call" | custom-call | tf_op jit(solution)/shard_map/pallas_call | solution.py:736
  52.0 1.1 %shard_map.69 = (bf16[1344,256]{1,0:T(8,128)(2,1)}, f32[336,384]{1,0:T(8,128)}) custom-call(bf16[1344,256]{1,0:T(8,128)(2,1)S(1)} %get-tuple-element.6.dx_in, f32[336,384]{1,0:T(8,128)S(1)} %get-tuple-element.7.dg_in), custom_call_target="tpu_custom_call" | custom-call | tf_op jit(solution)/shard_map/pallas_call | solution.py:766
